TPU v7x, 32 devices: a whole 2x2x4 slice. The times are simulated.
32 devices in a mesh: ep: 8 (over z, x), tp: 4 (over y, core).
Axes of the slice: x: 2, y: 2, z: 4, core: 2. Of those that a mesh axis runs over, the one named last changes fastest.
Arguments:
- x_in: bfloat16 [4096, 3072], P('tp', 'ep'), may hold values from -6 to 6
- z_in: bfloat16 [4096, 3072], P('tp', 'ep'), may hold values from -6 to 6
- dt_raw: float32 [64, 3072], P('tp', 'ep'), may hold values from -6 to 6
- decay_rate: float32 [64], P('tp'), may hold values from 0 to 1, as said below
- b_in: bfloat16 [256, 3072], P(None, 'ep'), may hold values from -6 to 6
- c_in: bfloat16 [256, 3072], P(None, 'ep'), may hold values from -6 to 6
- conv_x: float32 [4096, 4], P('tp'), may hold values from -3 to 3
- conv_b: float32 [256, 4], replicated, may hold values from -3 to 3
- conv_c: float32 [256, 4], replicated, may hold values from -3 to 3
- head_gain: float32 [4096], P('tp'), may hold values from 0.1 to 1.9
- moe_rows: bfloat16 [1280, 2048], P('ep'), may hold values from -6 to 6
- moe_gain: float32 [2048], replicated, may hold values from 0.1 to 1.9
- routes: int32 [1280, 2], P('ep'), may hold values from 0 to 7, all different within a row; in each aligned block of 160 rows (0 to 159, 160 to 319, ...) at most 80 rows name the same one
- route_logit: float32 [1280, 2], P('ep'), may hold values from -6 to 6
- w_gate: bfloat16 [8, 2048, 5120], P('ep', None, 'tp'), may hold values from -0.125 to 0.125
- w_up: bfloat16 [8, 2048, 5120], P('ep', None, 'tp'), may hold values from -0.125 to 0.125
- w_down: bfloat16 [8, 5120, 2048], P('ep', 'tp'), may hold values from -0.078125 to 0.078125
Outputs:
- mixed: bfloat16 [4096, 3072], P('tp', 'ep')
- moe_out: bfloat16 [2048, 1280], P('tp', 'ep')
Inputs may be any that keep to these rules, and one draw needn't show every extreme that they name: `routes`: each row names 2 different experts; among the rows of one index of ep no expert is named more than 80 times, a bound that some block reaches. `decay_rate`: positive rates.
All inputs are finite; a program needn't handle non-finite values.
Results may differ from a plain program's by a relative error of at most 0.018.
Values may be sent and summed in bfloat16 or wider, within the bound.
A program may use at most 64 MiB of HBM per device.

v0:
```python
import jax
import jax.numpy as jnp
from jax import lax
from jax.sharding import PartitionSpec as P

HEADS = 64
HEAD_DIM = 64
GROUPS = 2
NSTATE = 128
BLOCK = 128
EXP_DEV = 1


HIGHEST = lax.Precision.HIGHEST
ROW_EPS = 0.1
HEAD_EPS = 1.0


def from_behind(value, axis, steps):
    count = lax.axis_size(axis)
    initial, last = (max(0, -steps), min(count, count - steps))
    return lax.ppermute(value, axis, [(source, source + steps) for source in range(initial, last)])


def carried_in(shard, axis, join, neutral):
    place = lax.axis_index(axis)
    gathered = jax.tree.map(
        lambda a, kind: lax.all_gather(a.astype(kind), axis), shard, (jnp.bfloat16, jnp.bfloat16)
    )
    state = jax.tree.map(lambda a, e: jnp.zeros_like(a) + jnp.asarray(e, a.dtype), shard, neutral)

    def one(turn, state):
        return join(
            state,
            jax.tree.map(
                lambda a, own: lax.dynamic_index_in_dim(a, turn, 0, False).astype(own.dtype),
                gathered,
                shard,
            ),
        )

    return lax.fori_loop(0, place, one, state)


def conv_with_rims(signal, rim_rows, weight):
    taps = weight.shape[1]
    length = signal.shape[1]
    joined = jnp.concatenate([rim_rows.astype(jnp.float32), signal.astype(jnp.float32)], axis=1)
    running = jnp.zeros(signal.shape, jnp.float32)
    for offset in range(taps):
        running = running + weight[:, offset : offset + 1] * joined[:, offset : offset + length]
    return jax.nn.silu(running)


def block_step(state_in, x_block, b_block, c_block, log_block, step_block):
    cum_log = jnp.cumsum(log_block, axis=1)
    seg_log = cum_log[:, :, None] - cum_log[:, None, :]
    causal = jnp.tril(jnp.ones((log_block.shape[1], log_block.shape[1]), bool))
    decay_mask = jnp.exp(jnp.where(causal[None], seg_log, -jnp.inf))
    scores = (
        jnp.einsum("hnt,hns->hts", c_block, b_block, precision=HIGHEST)
        * decay_mask
        * step_block[:, None, :]
    )
    inner_term = jnp.einsum("hts,hps->hpt", scores, x_block, precision=HIGHEST)
    carried = (
        jnp.einsum("hnt,hpn->hpt", c_block, state_in, precision=HIGHEST)
        * jnp.exp(cum_log)[:, None, :]
    )
    tail_weight = jnp.exp(cum_log[:, -1:] - cum_log) * step_block
    fresh_state = jnp.einsum(
        "hps,hns->hpn", x_block * tail_weight[:, None, :], b_block, precision=HIGHEST
    )
    new_state = jnp.exp(cum_log[:, -1])[:, None, None] * state_in + fresh_state
    return (new_state, inner_term + carried)


def combine_states(before_part, after_part):
    return (
        before_part[0] * after_part[0],
        after_part[0][..., None, None] * before_part[1] + after_part[1],
    )


def mixer_half(x_in, z_in, dt_raw, decay_rate, b_in, c_in, conv_x, conv_b, conv_c, head_gain):
    head_count = dt_raw.shape[0]
    length = dt_raw.shape[1]
    taps = conv_x.shape[1]
    value_rows = x_in.shape[0]
    per_group = HEADS // GROUPS
    group_index = lax.axis_index("tp") * head_count // per_group
    b_own = lax.dynamic_slice_in_dim(b_in, group_index * NSTATE, NSTATE, 0)
    c_own = lax.dynamic_slice_in_dim(c_in, group_index * NSTATE, NSTATE, 0)
    taps_b = lax.dynamic_slice_in_dim(conv_b, group_index * NSTATE, NSTATE, 0)
    taps_c = lax.dynamic_slice_in_dim(conv_c, group_index * NSTATE, NSTATE, 0)
    edge = length - taps + 1
    own_rims = jnp.concatenate([x_in[:, edge:], b_own[:, edge:], c_own[:, edge:]], axis=0)
    rims = from_behind(own_rims, "ep", 1)
    x_conv = conv_with_rims(x_in, rims[:value_rows], conv_x).reshape(head_count, HEAD_DIM, length)
    b_conv = conv_with_rims(b_own, rims[value_rows : value_rows + NSTATE], taps_b)
    c_conv = conv_with_rims(c_own, rims[value_rows + NSTATE :], taps_c)
    step_dt = jax.nn.softplus(dt_raw)
    log_decay = -step_dt * decay_rate[:, None]
    block_count = length // BLOCK

    def blocks(tensor):
        return jnp.moveaxis(tensor.reshape(tensor.shape[:-1] + (block_count, BLOCK)), -2, 0)

    def spread_heads(tensor):
        return jnp.broadcast_to(tensor[None], (head_count,) + tensor.shape)

    def advance(state_in, inputs):
        x_block, b_block, c_block, log_block, step_block = inputs
        return block_step(
            state_in, x_block, spread_heads(b_block), spread_heads(c_block), log_block, step_block
        )

    init_state = jnp.zeros((head_count, HEAD_DIM, NSTATE), jnp.float32)
    local_state, block_out = lax.scan(
        advance,
        init_state,
        (blocks(x_conv), blocks(b_conv), blocks(c_conv), blocks(log_decay), blocks(step_dt)),
    )
    y_local = jnp.moveaxis(block_out, 0, -2).reshape(head_count, HEAD_DIM, length)
    total_decay = jnp.exp(jnp.sum(log_decay, axis=1))
    _, incoming = carried_in(
        (total_decay, local_state),
        "ep",
        combine_states,
        (jnp.ones_like(total_decay), jnp.zeros_like(local_state)),
    )
    reach_decay = jnp.exp(jnp.cumsum(log_decay, axis=1))
    carried = (
        jnp.einsum("nt,hpn->hpt", c_conv, incoming, precision=HIGHEST) * reach_decay[:, None, :]
    )
    y_mixed = y_local + carried
    gated_out = y_mixed * jax.nn.silu(
        z_in.astype(jnp.float32).reshape(head_count, HEAD_DIM, length)
    )
    head_scale = lax.rsqrt(jnp.mean(gated_out * gated_out, axis=1, keepdims=True) + HEAD_EPS)
    normed_out = gated_out * head_scale * head_gain.reshape(head_count, HEAD_DIM, 1)
    return normed_out.reshape(head_count * HEAD_DIM, length).astype(jnp.bfloat16)


def experts_half(moe_rows, moe_gain, routes, route_logit, w_gate, w_up, w_down):
    tokens = moe_rows.shape[0]
    top_count = routes.shape[1]
    features = moe_gain.shape[0]
    experts = EXP_DEV * lax.axis_size("ep")
    capacity = 2 * tokens * top_count // experts
    col_width = features // lax.axis_size("tp")
    rows_float = moe_rows.astype(jnp.float32)
    row_scale = lax.rsqrt(jnp.mean(rows_float * rows_float, axis=1, keepdims=True) + ROW_EPS)
    normed_float = rows_float * row_scale * moe_gain
    flat_routes = routes.reshape(-1)
    hit_table = (flat_routes[:, None] == jnp.arange(experts, dtype=jnp.int32)[None, :]).astype(
        jnp.int32
    )
    slot_rank = jnp.sum((jnp.cumsum(hit_table, axis=0) - hit_table) * hit_table, axis=1)
    slot_index = flat_routes * capacity + slot_rank
    owner_row = jnp.arange(tokens * top_count, dtype=jnp.int32) // top_count
    column = lax.axis_index("tp") * col_width
    normed = lax.dynamic_slice_in_dim(normed_float.astype(jnp.bfloat16), column, col_width, 1)
    outbox = (
        jnp.zeros((experts * capacity, col_width), jnp.bfloat16)
        .at[slot_index]
        .set(normed[owner_row])
    )
    arrived = lax.all_to_all(
        outbox.reshape(experts, capacity, col_width), "ep", split_axis=0, concat_axis=0, tiled=True
    ).reshape(-1, col_width)
    part_rows = lax.all_gather(arrived, "tp", axis=1, tiled=True)
    gate_rows = w_gate[0]
    up_rows = w_up[0]
    gate_act = jnp.dot(part_rows, gate_rows, preferred_element_type=jnp.float32)
    up_act = jnp.dot(part_rows, up_rows, preferred_element_type=jnp.float32)
    hidden = (jax.nn.silu(gate_act) * up_act).astype(jnp.bfloat16)
    columns = w_down[0]
    summed = lax.psum_scatter(
        lax.dot_general(
            columns, hidden, (((0,), (1,)), ((), ())), preferred_element_type=jnp.float32
        ).astype(jnp.bfloat16),
        "tp",
        scatter_dimension=0,
        tiled=True,
    )
    expert_out = summed.reshape(col_width, experts, capacity)
    returned = lax.all_to_all(expert_out, "ep", split_axis=1, concat_axis=1, tiled=True)
    picked = returned.reshape(col_width, experts * capacity)[:, slot_index].astype(jnp.float32)
    picked = picked.reshape(col_width, tokens, top_count)
    weight = jax.nn.sigmoid(route_logit - route_logit[:, ::-1])
    combined = jnp.sum(picked * weight[None], axis=2)
    return combined.astype(jnp.bfloat16)


def on_device(
    x_in,
    z_in,
    dt_raw,
    decay_rate,
    b_in,
    c_in,
    conv_x,
    conv_b,
    conv_c,
    head_gain,
    moe_rows,
    moe_gain,
    routes,
    route_logit,
    w_gate,
    w_up,
    w_down,
):
    mixed = mixer_half(
        x_in, z_in, dt_raw, decay_rate, b_in, c_in, conv_x, conv_b, conv_c, head_gain
    )
    moe_out = experts_half(moe_rows, moe_gain, routes, route_logit, w_gate, w_up, w_down)
    return (mixed, moe_out)


def solution(mesh):
    return jax.shard_map(
        on_device,
        mesh=mesh,
        in_specs=(
            P("tp", "ep"),
            P("tp", "ep"),
            P("tp", "ep"),
            P("tp"),
            P(None, "ep"),
            P(None, "ep"),
            P("tp", None),
            P(),
            P(),
            P("tp"),
            P("ep", None),
            P(),
            P("ep", None),
            P("ep", None),
            P("ep", None, "tp"),
            P("ep", None, "tp"),
            P("ep", "tp", None),
        ),
        out_specs=(P("tp", "ep"), P("tp", "ep")),
        check_vma=False,
    )
```

profile of v0, /device:TPU:24, one launch (start us, length us, event | category | flops | bytes accessed | tf_op | source)
XLA Modules:
  0.0 209.9 jit_solution(18337351531180557523)
XLA Ops:
  12.3 3.4 %scatter_custom_fusion = bf16[640,512]{1,0:T(8,128)(2,1)S(1)} fusion(s32[320]{0:T(512)S(1)} %get-tuple-element.186, bf16[160,512]{1,0:T(8,128)(2,1)S(1)} %fusion.45, s32[1024]{0:T(1024)S(1)} %pad_clamp_fusion.1, bf16[]{:T(256)} %constant.124.clone.1), kind=kCustom, calls=%fused_computation.70 | custom fusion | bytes 655362 | tf_op jit(solution)/shard_map/scatter | solution.py:167
  15.8 21.2 %all_to_all.10 = bf16[8,80,512]{2,1,0:T(8,128)(2,1)} all-to-all(bf16[8,80,512]{2,1,0:T(8,128)(2,1)S(1)} %bitcast.153), channel_id=1, replica_groups=mesh['ep'=8,'tp'=4] {'ep'}, dimensions={0} | all-to-all | bytes 1310720 | tf_op jit(solution)/shard_map/all_to_all | solution.py:169
  37.7 3.3 %collective-permute-start = (bf16[1280,3]{0,1:T(4,128)(2,1)S(1)}, bf16[1280,3]{0,1:T(4,128)(2,1)S(1)}, u32[]{:S(2)}, u32[]{:S(2)}) collective-permute-start(bf16[1280,3]{0,1:T(4,128)(2,1)S(1)} %pad_maximum_fusion.3), channel_id=1, source_target_pairs={{0,4},{4,8},{8,12},{12,16},{16,20},{20,24},{24,28},{1,5},{5,9},{9,... | collective-permute-start | bytes 23048 | tf_op jit(solution)/shard_map/ppermute | solution.py:22
  44.4 3.2 %divide_multiply_fusion = f32[1024,384]{1,0:T(8,128)} fusion(f32[1024,384]{1,0:T(8,128)S(1)} %convert_element_type.89, f32[1024,3]{1,0:T(8,128)S(1)} %copy.41, f32[1024]{0:T(1024)S(1)} %bitcast.164, f32[1024]{0:T(1024)S(1)} %bitcast.165, f32[1024]{0:T(1024)S(1)} %bitcast.163, f32[1024]{0:T(1024)S(1)} %bitcast.162), kind=kLoop, calls=%fused_computation.63 | loop fusion | flops 5505024 | bytes 3174400 | tf_op jit(solution)/shard_map/jit(silu)/mul | solution.py:52
  47.7 2.5 %reshape_reshape.3 = f32[16,64,3,128]{3,2,1,0:T(4,128)S(1)} reshape(f32[1024,384]{1,0:T(8,128)} %divide_multiply_fusion) | data formatting | bytes 3145728 | tf_op jit(solution)/shard_map/reshape;reshape | solution.py:107
  50.5 12.9 %all-gather.5.cloned.1.call-done = bf16[640,2048]{1,0:T(8,128)(2,1)} async-done(((bf16[640,512]{1,0:T(8,128)(2,1)}), bf16[640,2048]{1,0:T(8,128)(2,1)}) %all-gather.5.cloned.1.call-update) | async-done | bytes 2621456 | tf_op jit(solution)/shard_map/all_gather | solution.py:172
  63.4 8.5 %fusion.18 = f32[640,1280]{1,0:T(8,128)} fusion(bf16[640,2048]{1,0:T(8,128)(2,1)} %all-gather.5.cloned.1.call-done, bf16[1,2048,1280]{2,1,0:T(8,128)(2,1)} %param.35), kind=kOutput, calls=%fused_computation.35 | convolution fusion | flops 3355443200 | bytes 11141120 | tf_op jit(solution)/shard_map/dot_general | solution.py:175
  71.9 15.2 %fusion.29 = bf16[2048,640]{0,1:T(8,128)(2,1)} fusion(bf16[1,1280,2048]{2,1,0:T(8,128)(2,1)} %param.37, bf16[640,2048]{1,0:T(8,128)(2,1)} %all-gather.5.cloned.1.call-done, bf16[1,2048,1280]{2,1,0:T(8,128)(2,1)} %param.36, f32[640,1280]{1,0:T(8,128)} %fusion.18), kind=kOutput, calls=%fused_computation.40 | convolution fusion | flops 6717112320 | bytes 19005440 | tf_op jit(solution)/shard_map/dot_general | solution.py:180
  87.4 40.6 %while.26 = (s32[]{:T(128)}, f32[16,64,128]{2,1,0:T(8,128)S(1)}, f32[3,16,64,128]{3,2,1,0:T(8,128)}, f32[3,16,128]{2,0,1:T(4,128)S(1)}, f32[3,16,64,128]{3,0,2,1...) while((s32[]{:T(128)}, f32[16,64,128]{2,1,0:T(8,128)S(1)}, ...), condition=%wide.region_2.3_spmd.clone, body=%wide.region_0.2_spmd.clone.sunk | while | flops 1008879616 | bytes 10045104 | solution.py:119
  87.4 1.4 constant_dynamic-slice_fusion.14
  90.7 1.6 fusion.104
  92.5 2.7 %fusion.105 = f32[16,128,128]{2,1,0:T(8,128)S(1)} fusion(f32[16,128]{1,0:T(8,128)} %bitcast.142, f32[16,128]{1,0:T(8,128)S(1)} %reduce_window_sum.51, f32[128,128]{1,0:T(8,128)S(1)} %bitcast.151, f32[128,128]{1,0:T(8,128)S(1)} %bitcast.148, pred[128,128]{1,0:T(8,128)(4,1)S(1)} %iota_compare_fusion.4), kind=kOutput, calls=%fused_computation.6.clone.1 | convolution fusion | flops 403701760 | bytes 1212416 | tf_op jit(solution)/shard_map/while/body/eval_jaxpr/hnt,hns->hts/dot_general | solution.py:61
  95.8 3.0 %fusion.106 = f32[3,16,64,128]{3,2,1,0:T(8,128)} fusion(f32[3,16,64,128]{3,2,1,0:T(8,128)} %get-tuple-element.298, s32[]{:T(128)} %get-tuple-element.296, f32[16,64,128]{2,1,0:T(8,128)S(1)} %fusion.104, f32[16,64,128]{2,1,0:T(8,128)S(1)} %bitcast.144, f32[16,128,128]{2,1,0:T(8,128)S(1)} %fusion.105), kind=kOutput, calls=%fused_computation.11.clone.1 | convolution fusion | flops 201457664 | bytes 2621952 | tf_op jit(solution)/shard_map/while/body/eval_jaxpr/hts,hps->hpt/dot_general | solution.py:65
  98.8 2.1 %convolution_add_fusion.3 = f32[16,64,128]{2,1,0:T(8,128)S(1)} fusion(f32[128,128]{1,0:T(8,128)S(1)} %bitcast.149, f32[16,64,128]{2,1,0:T(8,128)S(1)} %bitcast.145, f32[16,64,128]{2,1,0:T(8,128)S(1)} %get-tuple-element.297, f32[16,128]{1,0:T(8,128)S(1)} %get-tuple-element.282, f32[16]{0:T(128)S(1)} %exp.118, pred[]{:T(512)S(6)} %compare.10), kind=kOutput, calls=%fused_computation.12.clone.1 | convolution fusion | flops 201850880 | bytes 1646657 | tf_op jit(solution)/shard_map/while/body/eval_jaxpr/hps,hns->hpn/dot_general | solution.py:71
  101.0 1.4 constant_dynamic-slice_fusion.14
  104.3 1.7 fusion.104
  106.1 2.7 %fusion.105 = f32[16,128,128]{2,1,0:T(8,128)S(1)} fusion(f32[16,128]{1,0:T(8,128)} %bitcast.142, f32[16,128]{1,0:T(8,128)S(1)} %reduce_window_sum.51, f32[128,128]{1,0:T(8,128)S(1)} %bitcast.151, f32[128,128]{1,0:T(8,128)S(1)} %bitcast.148, pred[128,128]{1,0:T(8,128)(4,1)S(1)} %iota_compare_fusion.4), kind=kOutput, calls=%fused_computation.6.clone.1 | convolution fusion | flops 403701760 | bytes 1212416 | tf_op jit(solution)/shard_map/while/body/eval_jaxpr/hnt,hns->hts/dot_general | solution.py:61
  109.4 3.0 %fusion.106 = f32[3,16,64,128]{3,2,1,0:T(8,128)} fusion(f32[3,16,64,128]{3,2,1,0:T(8,128)} %get-tuple-element.298, s32[]{:T(128)} %get-tuple-element.296, f32[16,64,128]{2,1,0:T(8,128)S(1)} %fusion.104, f32[16,64,128]{2,1,0:T(8,128)S(1)} %bitcast.144, f32[16,128,128]{2,1,0:T(8,128)S(1)} %fusion.105), kind=kOutput, calls=%fused_computation.11.clone.1 | convolution fusion | flops 201457664 | bytes 2621952 | tf_op jit(solution)/shard_map/while/body/eval_jaxpr/hts,hps->hpt/dot_general | solution.py:65
  112.4 2.1 %convolution_add_fusion.3 = f32[16,64,128]{2,1,0:T(8,128)S(1)} fusion(f32[128,128]{1,0:T(8,128)S(1)} %bitcast.149, f32[16,64,128]{2,1,0:T(8,128)S(1)} %bitcast.145, f32[16,64,128]{2,1,0:T(8,128)S(1)} %get-tuple-element.297, f32[16,128]{1,0:T(8,128)S(1)} %get-tuple-element.282, f32[16]{0:T(128)S(1)} %exp.118, pred[]{:T(512)S(6)} %compare.10), kind=kOutput, calls=%fused_computation.12.clone.1 | convolution fusion | flops 201850880 | bytes 1646657 | tf_op jit(solution)/shard_map/while/body/eval_jaxpr/hps,hns->hpn/dot_general | solution.py:71
  114.5 1.4 constant_dynamic-slice_fusion.14
  117.9 1.6 fusion.104
  119.6 2.7 %fusion.105 = f32[16,128,128]{2,1,0:T(8,128)S(1)} fusion(f32[16,128]{1,0:T(8,128)} %bitcast.142, f32[16,128]{1,0:T(8,128)S(1)} %reduce_window_sum.51, f32[128,128]{1,0:T(8,128)S(1)} %bitcast.151, f32[128,128]{1,0:T(8,128)S(1)} %bitcast.148, pred[128,128]{1,0:T(8,128)(4,1)S(1)} %iota_compare_fusion.4), kind=kOutput, calls=%fused_computation.6.clone.1 | convolution fusion | flops 403701760 | bytes 1212416 | tf_op jit(solution)/shard_map/while/body/eval_jaxpr/hnt,hns->hts/dot_general | solution.py:61
  122.9 2.9 %fusion.106 = f32[3,16,64,128]{3,2,1,0:T(8,128)} fusion(f32[3,16,64,128]{3,2,1,0:T(8,128)} %get-tuple-element.298, s32[]{:T(128)} %get-tuple-element.296, f32[16,64,128]{2,1,0:T(8,128)S(1)} %fusion.104, f32[16,64,128]{2,1,0:T(8,128)S(1)} %bitcast.144, f32[16,128,128]{2,1,0:T(8,128)S(1)} %fusion.105), kind=kOutput, calls=%fused_computation.11.clone.1 | convolution fusion | flops 201457664 | bytes 2621952 | tf_op jit(solution)/shard_map/while/body/eval_jaxpr/hts,hps->hpt/dot_general | solution.py:65
  125.9 2.1 %convolution_add_fusion.3 = f32[16,64,128]{2,1,0:T(8,128)S(1)} fusion(f32[128,128]{1,0:T(8,128)S(1)} %bitcast.149, f32[16,64,128]{2,1,0:T(8,128)S(1)} %bitcast.145, f32[16,64,128]{2,1,0:T(8,128)S(1)} %get-tuple-element.297, f32[16,128]{1,0:T(8,128)S(1)} %get-tuple-element.282, f32[16]{0:T(128)S(1)} %exp.118, pred[]{:T(512)S(6)} %compare.10), kind=kOutput, calls=%fused_computation.12.clone.1 | convolution fusion | flops 201850880 | bytes 1646657 | tf_op jit(solution)/shard_map/while/body/eval_jaxpr/hps,hns->hpn/dot_general | solution.py:71
  128.8 1.3 dynamic-slice
  131.7 17.1 %all-reduce.1 = bf16[128]{0:T(256)(128)(2,1)S(1)} all-reduce(bf16[128]{0:T(256)(128)(2,1)S(1)} %dynamic-update-slice), channel_id=2, replica_groups=mesh['ep'=8,'tp'=4] {'ep'}, use_global_device_ids=true, to_apply=%add.1 | all-reduce | flops 128 | bytes 512
  153.7 8.6 %all-to-all-start.1 = ((bf16[512,8,80]{0,2,1:T(8,128)(2,1)}), bf16[512,8,80]{0,2,1:T(8,128)(2,1)S(1)}, u32[]{:S(2)}, u32[]{:S(2)}) async-start(bf16[512,8,80]{0,2,1:T(8,128)(2,1)} %bitcast.160), calls=%async_computation.2 | async-start | bytes 1310720 | tf_op jit(solution)/shard_map/all_to_all | solution.py:188
  162.3 24.8 %all-gather.7.cloned.1.call-done = bf16[128,64,128]{2,1,0:T(8,128)(2,1)} async-done(((bf16[16,64,128]{2,1,0:T(8,128)(2,1)}), bf16[128,64,128]{2,1,0:T(8,128)(2,1)}) %all-gather.7.cloned.1.call-update) | async-done | bytes 2097168 | tf_op jit(solution)/shard_map/all_gather | solution.py:28
  187.2 7.0 %while.25 = (s32[]{:T(128)}, f32[16,64,128]{2,1,0:T(8,128)S(1)}, s32[]{:T(128)}, bf16[8,16]{1,0:T(8,128)(2,1)S(1)}, bf16[8,16,64,128]{3,2,1,0:T(8,128)(2,1)}, /*index=5*/s32[]{:T(128)}, s32[]{:T(128)}, s32[]{:T(128)}) while((s32[]{:T(128)}, f32[16,64,128]{2,1,0:T(8,128)S(1)}, s32[]{:T(128)}, bf16[8,16]{1,0:T(8,128)(2,1)S(1)}, ...), condition=%wide.region_5.6_spmd, body=%wide.region_4.5_spmd.sunk | while | flops 393237 | bytes 1311007 | solution.py:42
  194.3 3.0 %multiply_reduce_fusion = (f32[16,384]{1,0:T(8,128)S(1)}, f32[16,64,384]{2,1,0:T(8,128)S(1)}) fusion(bf16[16,64,384]{2,1,0:T(8,128)(2,1)} %bitcast.168, f32[16,384]{1,0:T(8,128)S(1)} %copy_bitcast_fusion, f32[16,64,128]{2,1,0:T(8,128)S(1)} %get-tuple-element.91, f32[128,384]{0,1:T(8,128)S(1)} %bitcast.155, f32[3,16,64,128]{3,2,1,0:T(8,128)S(1)} %copy-done.20), kind=kOutput, calls=%fused_computation.62 | convolution fusion | flops 607905792 | bytes 4702208 | tf_op jit(solution)/shard_map/nt,hpn->hpt/dot_general | solution.py:134
  198.5 2.0 gather_fusion
  201.0 1.5 multiply_reduce_fusion.2
  (178 shorter events, 31.3 us)
Async XLA Ops:
  8.0 55.4 %all-gather.5.cloned.1.call-start = ((), (), s32[]{:S(2)}) async-start(), calls=%async_computation.3 | async-start | bytes 3276800 | tf_op jit(solution)/shard_map/all_gather | solution.py:172
  11.4 25.7 %copy-start.13 = (s32[320]{0:T(512)}, s32[320]{0:T(512)S(1)}, u32[]{:S(2)}) copy-start(s32[320]{0:T(512)S(1)} %get-tuple-element.186) | copy-start | bytes 3844
  12.2 24.9 %copy-start.9 = (bf16[256,384]{1,0:T(8,128)(2,1)S(1)}, bf16[256,384]{1,0:T(8,128)(2,1)}, u32[]{:S(2)}) copy-start(bf16[256,384]{1,0:T(8,128)(2,1)} %param.26) | copy-start | bytes 589828
  12.2 24.9 %copy-start.10 = (bf16[256,384]{1,0:T(8,128)(2,1)S(1)}, bf16[256,384]{1,0:T(8,128)(2,1)}, u32[]{:S(2)}) copy-start(bf16[256,384]{1,0:T(8,128)(2,1)} %param.25) | copy-start | bytes 589828
  12.3 25.1 %copy-start.1 = (bf16[1024,384]{1,0:T(8,128)(2,1)S(1)}, bf16[1024,384]{1,0:T(8,128)(2,1)}, u32[]{:S(2)}) copy-start(bf16[1024,384]{1,0:T(8,128)(2,1)} %param.21) | copy-start | bytes 2359300
  15.7 25.4 %copy-start.17 = (f32[256,4]{0,1:T(4,128)S(1)}, f32[256,4]{0,1:T(4,128)}, u32[]{:S(2)}) copy-start(f32[256,4]{0,1:T(4,128)} %param.29) | copy-start | bytes 12292
  15.7 25.4 %copy-start.18 = (f32[256,4]{0,1:T(4,128)S(1)}, f32[256,4]{0,1:T(4,128)}, u32[]{:S(2)}) copy-start(f32[256,4]{0,1:T(4,128)} %param.28) | copy-start | bytes 12292
  15.7 25.4 %copy-start.12 = (f32[1024,4]{0,1:T(4,128)S(1)}, f32[1024,4]{0,1:T(4,128)}, u32[]{:S(2)}) copy-start(f32[1024,4]{0,1:T(4,128)} %param.27) | copy-start | bytes 49156
  15.7 25.4 %copy-start.11 = (f32[16,384]{1,0:T(8,128)S(1)}, f32[16,384]{1,0:T(8,128)}, u32[]{:S(2)}) copy-start(f32[16,384]{1,0:T(8,128)} %param.23) | copy-start | bytes 73732
  15.7 25.4 %copy-start.19 = (f32[16]{0:T(128)S(1)}, f32[16]{0:T(128)}, u32[]{:S(2)}) copy-start(f32[16]{0:T(128)} %param.24) | copy-start | bytes 196
  37.0 116.7 %reduce-scatter.2.cloned.1.call-start = ((), (), s32[]{:S(2)}) async-start(), calls=%async_computation.4 | async-start | bytes 3276800 | tf_op jit(solution)/shard_map/reduce_scatter | solution.py:179
  37.7 6.5 %collective-permute-start = (bf16[1280,3]{0,1:T(4,128)(2,1)S(1)}, bf16[1280,3]{0,1:T(4,128)(2,1)S(1)}, u32[]{:S(2)}, u32[]{:S(2)}) collective-permute-start(bf16[1280,3]{0,1:T(4,128)(2,1)S(1)} %pad_maximum_fusion.3), channel_id=1, source_target_pairs={{0,4},{4,8},{8,12},{12,16},{16,20},{20,24},{24,28},{1,5},{5,9},{9,... | collective-permute-start | bytes 23048 | tf_op jit(solution)/shard_map/ppermute | solution.py:22
  41.9 2.6 %copy-start.4 = (f32[16,384]{1,0:T(8,128)}, f32[16,384]{1,0:T(8,128)S(1)}, u32[]{:S(2)}) copy-start(f32[16,384]{1,0:T(8,128)S(1)} %get-tuple-element.162) | copy-start | bytes 73732
  47.7 2.7 %copy-start.15 = (f32[128]{0:T(128)S(1)}, f32[128]{0:T(128)}, u32[]{:S(2)}) copy-start(f32[128]{0:T(128)} %get-tuple-element.178) | copy-start | bytes 1540
  47.7 2.7 %copy-start.16 = (f32[128]{0:T(128)S(1)}, f32[128]{0:T(128)}, u32[]{:S(2)}) copy-start(f32[128]{0:T(128)} %get-tuple-element.179) | copy-start | bytes 1540
  87.1 100.0 %all-gather.7.cloned.1.call-start = ((), (), s32[]{:S(2)}) async-start(), calls=%async_computation.5 | async-start | bytes 2359296 | tf_op jit(solution)/shard_map/all_gather | solution.py:28
  87.4 3.2 %copy-start.5 = (f32[3,16,128]{2,0,1:T(4,128)}, f32[3,16,128]{2,0,1:T(4,128)S(1)}, u32[]{:S(2)}) copy-start(f32[3,16,128]{2,0,1:T(4,128)S(1)} %get-tuple-element.310) | copy-start | bytes 73732 | tf_op jit(solution)/shard_map/while
  87.4 3.3 %copy-start.2 = (f32[3,128,128]{1,2,0:T(8,128)}, f32[3,128,128]{1,2,0:T(8,128)S(1)}, u32[]{:S(2)}) copy-start(f32[3,128,128]{1,2,0:T(8,128)S(1)} %get-tuple-element.313) | copy-start | bytes 589828 | tf_op jit(solution)/shard_map/while
  95.8 3.0 %copy-start.8 = (f32[16]{0:T(128)S(1)}, f32[16]{0:T(128)}, u32[]{:S(2)}) copy-start(f32[16]{0:T(128)} %copy-done.7) | copy-start | bytes 196 | tf_op jit(solution)/shard_map/while
  95.8 5.1 %copy-start.6 = (f32[3,16,128]{2,0,1:T(4,128)S(1)}, f32[3,16,128]{2,0,1:T(4,128)}, u32[]{:S(2)}) copy-start(f32[3,16,128]{2,0,1:T(4,128)} %copy-done.5) | copy-start | bytes 73732 | tf_op jit(solution)/shard_map/while
  98.8 2.2 %copy-start.3 = (f32[3,128,128]{1,2,0:T(8,128)S(1)}, f32[3,128,128]{1,2,0:T(8,128)}, u32[]{:S(2)}) copy-start(f32[3,128,128]{1,2,0:T(8,128)} %copy-done.2) | copy-start | bytes 589828 | tf_op jit(solution)/shard_map/while
  101.0 3.2 %copy-start.5 = (f32[3,16,128]{2,0,1:T(4,128)}, f32[3,16,128]{2,0,1:T(4,128)S(1)}, u32[]{:S(2)}) copy-start(f32[3,16,128]{2,0,1:T(4,128)S(1)} %get-tuple-element.310) | copy-start | bytes 73732 | tf_op jit(solution)/shard_map/while
  101.0 3.3 %copy-start.2 = (f32[3,128,128]{1,2,0:T(8,128)}, f32[3,128,128]{1,2,0:T(8,128)S(1)}, u32[]{:S(2)}) copy-start(f32[3,128,128]{1,2,0:T(8,128)S(1)} %get-tuple-element.313) | copy-start | bytes 589828 | tf_op jit(solution)/shard_map/while
  109.4 3.0 %copy-start.8 = (f32[16]{0:T(128)S(1)}, f32[16]{0:T(128)}, u32[]{:S(2)}) copy-start(f32[16]{0:T(128)} %copy-done.7) | copy-start | bytes 196 | tf_op jit(solution)/shard_map/while
  109.4 5.1 %copy-start.6 = (f32[3,16,128]{2,0,1:T(4,128)S(1)}, f32[3,16,128]{2,0,1:T(4,128)}, u32[]{:S(2)}) copy-start(f32[3,16,128]{2,0,1:T(4,128)} %copy-done.5) | copy-start | bytes 73732 | tf_op jit(solution)/shard_map/while
  114.5 3.2 %copy-start.5 = (f32[3,16,128]{2,0,1:T(4,128)}, f32[3,16,128]{2,0,1:T(4,128)S(1)}, u32[]{:S(2)}) copy-start(f32[3,16,128]{2,0,1:T(4,128)S(1)} %get-tuple-element.310) | copy-start | bytes 73732 | tf_op jit(solution)/shard_map/while
  114.5 3.3 %copy-start.2 = (f32[3,128,128]{1,2,0:T(8,128)}, f32[3,128,128]{1,2,0:T(8,128)S(1)}, u32[]{:S(2)}) copy-start(f32[3,128,128]{1,2,0:T(8,128)S(1)} %get-tuple-element.313) | copy-start | bytes 589828 | tf_op jit(solution)/shard_map/while
  122.9 3.0 %copy-start.8 = (f32[16]{0:T(128)S(1)}, f32[16]{0:T(128)}, u32[]{:S(2)}) copy-start(f32[16]{0:T(128)} %copy-done.7) | copy-start | bytes 196 | tf_op jit(solution)/shard_map/while
  122.9 5.1 %copy-start.6 = (f32[3,16,128]{2,0,1:T(4,128)S(1)}, f32[3,16,128]{2,0,1:T(4,128)}, u32[]{:S(2)}) copy-start(f32[3,16,128]{2,0,1:T(4,128)} %copy-done.5) | copy-start | bytes 73732 | tf_op jit(solution)/shard_map/while
  125.9 2.2 %copy-start.3 = (f32[3,128,128]{1,2,0:T(8,128)S(1)}, f32[3,128,128]{1,2,0:T(8,128)}, u32[]{:S(2)}) copy-start(f32[3,128,128]{1,2,0:T(8,128)} %copy-done.2) | copy-start | bytes 589828 | tf_op jit(solution)/shard_map/while
  153.7 44.8 %all-to-all-start.1 = ((bf16[512,8,80]{0,2,1:T(8,128)(2,1)}), bf16[512,8,80]{0,2,1:T(8,128)(2,1)S(1)}, u32[]{:S(2)}, u32[]{:S(2)}) async-start(bf16[512,8,80]{0,2,1:T(8,128)(2,1)} %bitcast.160), calls=%async_computation.2 | async-start | bytes 1310720 | tf_op jit(solution)/shard_map/all_to_all | solution.py:188
  187.2 7.1 %copy-start.20 = (f32[3,16,64,128]{3,2,1,0:T(8,128)S(1)}, f32[3,16,64,128]{3,2,1,0:T(8,128)}, u32[]{:S(2)}) copy-start(f32[3,16,64,128]{3,2,1,0:T(8,128)} %get-tuple-element.89) | copy-start | bytes 4718596
  (6 other events, 9.0 us)
Sparse Core Ops, SparseCore 0:
  37.1 26.2 all-gather.4
  87.2 34.3 reduce-scatter.1
Sparse Core Ops, SparseCore 1:
  128.9 58.2 all-gather.6
where the time goes:
time: 213 us; the launch traced here: 210 us
  matrix products  55.1 us (26%)
  waiting for transfers between devices  38.7 us (18%)
  blocking collectives  38.3 us (18%)
  other arithmetic  25 us (12%)
  local copies, waits for them, and re-layouts  23.1 us (11%)
  between operations  16.7 us (8%)
  starting transfers between devices  12.3 us (6%)
    all_gather x1, waiting for transfers between devices, carried_in(): lax.all_gather(a.astype(kind), axis)  24.8 us
    all_to_all x1, blocking collectives, experts_half(): lax.all_to_all(outbox.reshape(experts, capacity, col_width), 'ep', split_...  21.2 us
    unnamed x1, blocking collectives  17.1 us
    dot_general x1, matrix products, experts_half(): lax.dot_general(columns, hidden, (((0,), (1,)), ((), ())), preferred_elem...  15.2 us
    all_gather x1, waiting for transfers between devices, experts_half(): part_rows = lax.all_gather(arrived, 'tp', axis=1, tiled=True)  12.9 us
    dot_general x3, matrix products, block_step(): inner_term = jnp.einsum('hts,hps->hpt', scores, x_block, precision=HIGHEST)  8.92 us
    all_to_all x1, starting transfers between devices, experts_half(): lax.all_to_all(expert_out, 'ep', split_axis=1, concat_axis=1, tiled=True)  8.64 us
    dot_general x1, matrix products, experts_half(): gate_act = jnp.dot(part_rows, gate_rows, preferred_element_type=jnp.float32)  8.51 us
  transfers between devices with their start and end apart: 5, of which 3 were waited for; matrix products, arithmetic and copies ran while one was open for 32% of the time, Pallas kernels for 0%

commit v1 on v0

v1 whole, which is shorter than its diff:
```python
import functools
import jax
import jax.numpy as jnp
from jax import lax
from jax.experimental import pallas as pl
from jax.experimental.pallas import tpu as pltpu
from jax.sharding import PartitionSpec as P

HEADS = 64
HEAD_DIM = 64
GROUPS = 2
NSTATE = 128
BLOCK = 128
ROW_EPS = 0.1
HEAD_EPS = 1.0
LANES = 128
F32 = jnp.float32
BF16 = jnp.bfloat16
VMEM = pltpu.VMEM


def vmem_specs(count):
    return [pl.BlockSpec(memory_space=VMEM)] * count


def cost(flops, moved):
    return pl.CostEstimate(flops=flops, bytes_accessed=moved, transcendentals=0)


def dot(a, b, dims, precision=None):
    return lax.dot_general(a, b, (dims, ((), ())), preferred_element_type=F32, precision=precision)


def silu(v):
    return v / (1.0 + jnp.exp(-v))


def conv_rows(signal, rim, weight):
    taps = weight.shape[1]
    joined = jnp.concatenate([rim.astype(F32), signal.astype(F32)], axis=1)
    running = weight[:, taps - 1 : taps] * joined[:, LANES:]
    for back in range(1, taps):
        moved = pltpu.roll(joined, back, 1)[:, LANES:]
        running = running + weight[:, taps - 1 - back : taps - back] * moved
    return silu(running)


def prefix_decays(dt_ref, rate_ref):
    dt = dt_ref[...]
    step = jnp.maximum(dt, 0.0) + jnp.log1p(jnp.exp(-jnp.abs(dt)))
    log_decay = -step * rate_ref[...]
    length = dt.shape[1]
    row = lax.broadcasted_iota(jnp.int32, (length, length), 0)
    col = lax.broadcasted_iota(jnp.int32, (length, length), 1)
    upper = jnp.where(row <= col, 1.0, 0.0).astype(F32)
    lower = jnp.where(row >= col, 1.0, 0.0).astype(F32)
    high = lax.Precision.HIGHEST
    cum = dot(log_decay, upper, ((1,), (0,)), high)
    cum_col = dot(lower, log_decay, ((1,), (1,)), high)
    return step, cum, cum_col


def span_kernel(
    x_ref, rim_ref, tapx_ref, b_ref, brim_ref, tapb_ref, c_ref, crim_ref, tapc_ref, dt_ref, rate_ref,
    y_ref, state_ref, conv_ref, cum_ref, reach_ref, step_ref, col_ref, score_ref, bconv_ref,
):
    heads, length = dt_ref.shape
    step, cum, cum_col = prefix_decays(dt_ref, rate_ref)
    step_ref[...] = step
    cum_ref[...] = cum
    reach_ref[...] = jnp.exp(cum[:, length - 1 :])
    b_conv = conv_rows(b_ref[...], brim_ref[...], tapb_ref[...]).astype(BF16)
    c_conv = conv_rows(c_ref[...], crim_ref[...], tapc_ref[...]).astype(BF16)
    bconv_ref[...] = b_conv
    conv_ref[...] = c_conv
    score_ref[...] = dot(b_conv, c_conv, ((0,), (0,)))
    row = lax.broadcasted_iota(jnp.int32, (BLOCK, BLOCK), 0)
    col = lax.broadcasted_iota(jnp.int32, (BLOCK, BLOCK), 1)
    causal = row <= col
    for head in range(heads):
        col_ref[head] = jnp.broadcast_to(cum_col[:, head : head + 1], (length, LANES))

    def one(head, carry):
        rows = pl.ds(pl.multiple_of(head * HEAD_DIM, HEAD_DIM), HEAD_DIM)
        x = conv_rows(x_ref[rows, :], rim_ref[rows, :], tapx_ref[rows, :])
        own = cum_ref[pl.ds(head, 1), :]
        xs = x * step_ref[pl.ds(head, 1), :]
        tail = xs * jnp.exp(own[:, length - 1 :] - own)
        state_ref[rows, :] = dot(tail.astype(BF16), bconv_ref[...], ((1,), (1,)))
        xs = xs.astype(BF16)
        for target in range(length // BLOCK):
            at = slice(target * BLOCK, (target + 1) * BLOCK)
            pieces = []
            for source in range(target + 1):
                of = slice(source * BLOCK, (source + 1) * BLOCK)
                gap = own[:, at] - col_ref[head, of, :]
                if source == target:
                    gap = jnp.where(causal, gap, -jnp.inf)
                pieces.append((score_ref[of, at] * jnp.exp(gap)).astype(BF16))
            mask = pieces[0] if target == 0 else jnp.concatenate(pieces, axis=0)
            y_ref[rows, at] = dot(xs[:, : (target + 1) * BLOCK], mask, ((1,), (0,)))
        return carry

    lax.fori_loop(0, heads, one, 0)


def close_kernel(y_ref, state_ref, conv_ref, cum_ref, z_ref, gain_ref, out_ref):
    heads = cum_ref.shape[0]

    def one(head, carry):
        rows = pl.ds(pl.multiple_of(head * HEAD_DIM, HEAD_DIM), HEAD_DIM)
        carried = dot(state_ref[rows, :].astype(BF16), conv_ref[...], ((1,), (0,)))
        y = y_ref[rows, :] + carried * jnp.exp(cum_ref[pl.ds(head, 1), :])
        gated = y * silu(z_ref[rows, :].astype(F32))
        scale = lax.rsqrt(jnp.mean(gated * gated, axis=0, keepdims=True) + HEAD_EPS)
        out_ref[rows, :] = (gated * scale * gain_ref[rows, :]).astype(BF16)
        return carry

    lax.fori_loop(0, heads, one, 0)


def outbox_kernel(rows_ref, gain_ref, routes_ref, logit_ref, out_ref, pick_ref, *, experts, capacity):
    width = out_ref.shape[1]
    tokens = rows_ref.shape[0]
    values = rows_ref[...].astype(F32)
    scale = lax.rsqrt(jnp.mean(values * values, axis=1, keepdims=True) + ROW_EPS)
    column = pl.ds(pl.multiple_of(lax.axis_index("tp") * width, LANES), width)
    normed = (rows_ref[:, column].astype(F32) * scale * gain_ref[:, column]).astype(BF16)
    routes = routes_ref[...]
    logit = logit_ref[...]
    first = 1.0 / (1.0 + jnp.exp(logit[1:2] - logit[0:1]))
    second = 1.0 / (1.0 + jnp.exp(logit[0:1] - logit[1:2]))
    number = lax.broadcasted_iota(jnp.int32, (experts, tokens), 0)
    in_first = number == routes[0:1]
    in_second = number == routes[1:2]
    hits = jnp.where(in_first, 1.0, 0.0) + jnp.where(in_second, 1.0, 0.0)
    row = lax.broadcasted_iota(jnp.int32, (tokens, tokens), 0)
    col = lax.broadcasted_iota(jnp.int32, (tokens, tokens), 1)
    earlier = jnp.where(row < col, 1.0, 0.0).astype(BF16)
    rank = dot(hits.astype(BF16), earlier, ((1,), (0,)))
    weight = jnp.where(in_first, first, 0.0) + jnp.where(in_second, second, 0.0)
    slot = jnp.where(hits > 0.0, number * capacity + rank.astype(jnp.int32), -1)
    place = lax.broadcasted_iota(jnp.int32, (experts * capacity, tokens), 0)
    chosen = jnp.zeros((experts * capacity, tokens), F32)
    weighed = jnp.zeros((experts * capacity, tokens), F32)
    for expert in range(experts):
        same = place == slot[expert : expert + 1]
        chosen = jnp.where(same, 1.0, chosen)
        weighed = jnp.where(same, weight[expert : expert + 1], weighed)
    pick_ref[...] = weighed.astype(BF16)
    out_ref[...] = dot(chosen.astype(BF16), normed, ((1,), (0,))).astype(BF16)


def ffn_kernel(parts, *refs):
    pieces = refs[:parts]
    gate_ref, up_ref, down_ref = refs[parts : parts + 3]
    outs = refs[parts + 3 : 2 * parts + 3]
    joined, total = refs[2 * parts + 3 :]
    me = lax.axis_index("tp")
    width = pieces[0].shape[1]
    turn = pl.program_id(0)

    def column(part):
        return pl.ds(pl.multiple_of((me ^ part) * width, LANES), width)

    @pl.when(turn == 0)
    def _():
        for part in range(parts):
            joined[:, column(part)] = pieces[part][...]

    gate = dot(joined[...], gate_ref[0], ((1,), (0,)))
    up = dot(joined[...], up_ref[0], ((1,), (0,)))
    hidden = (silu(gate) * up).astype(BF16)
    partial = dot(hidden, down_ref[0], ((1,), (0,)))

    @pl.when(turn == 0)
    def _():
        total[...] = partial

    @pl.when(turn > 0)
    def _():
        total[...] += partial

    @pl.when(turn == pl.num_programs(0) - 1)
    def _():
        for part in range(parts):
            outs[part][...] = total[:, column(part)].astype(BF16)


def combine_kernel(back_ref, pick_ref, out_ref):
    out_ref[...] = dot(back_ref[...], pick_ref[...], ((0,), (0,))).astype(BF16)


def from_behind(value, axis, steps):
    count = lax.axis_size(axis)
    return lax.ppermute(value, axis, [(source, source + steps) for source in range(count - steps)])


def swap(value, axis, bit):
    count = lax.axis_size(axis)
    return lax.ppermute(value, axis, [(source, source ^ bit) for source in range(count)])


def on_device(
    x_in, z_in, dt_raw, decay_rate, b_in, c_in, conv_x, conv_b, conv_c, head_gain,
    moe_rows, moe_gain, routes, route_logit, w_gate, w_up, w_down,
):
    heads, length = dt_raw.shape
    value_rows = x_in.shape[0]
    taps = conv_x.shape[1]
    tp_size = lax.axis_size("tp")
    ep_size = lax.axis_size("ep")
    tokens, features = moe_rows.shape
    top = routes.shape[1]
    experts = ep_size
    capacity = 2 * tokens * top // experts
    width = features // tp_size
    slots = experts * capacity

    outbox, pick = pl.pallas_call(
        functools.partial(outbox_kernel, experts=experts, capacity=capacity),
        out_shape=(
            jax.ShapeDtypeStruct((slots, width), BF16),
            jax.ShapeDtypeStruct((slots, tokens), BF16),
        ),
        in_specs=vmem_specs(4),
        out_specs=tuple(vmem_specs(2)),
        name="outbox",
        cost_estimate=cost(2 * slots * tokens * width, 2 * tokens * features),
    )(moe_rows, moe_gain.reshape(1, features), routes.T, route_logit.T)
    arrived = lax.all_to_all(
        outbox.reshape(experts, capacity, width), "ep", split_axis=0, concat_axis=0, tiled=True
    ).reshape(slots, width)

    group = lax.axis_index("tp") * heads // (HEADS // GROUPS)

    def of_group(tensor):
        return lax.dynamic_slice_in_dim(tensor, group * NSTATE, NSTATE, 0)

    b_own, c_own, taps_b, taps_c = map(of_group, (b_in, c_in, conv_b, conv_c))
    edge = length - taps + 1
    ends = jnp.concatenate([x_in[:, edge:], b_own[:, edge:], c_own[:, edge:]], axis=0)
    rims = from_behind(ends.T, "ep", 1).T
    rims = jnp.pad(rims, ((0, 0), (LANES - taps + 1, 0)))
    y_local, state, c_conv, cum, reach = pl.pallas_call(
        span_kernel,
        out_shape=(
            jax.ShapeDtypeStruct((value_rows, length), F32),
            jax.ShapeDtypeStruct((value_rows, NSTATE), F32),
            jax.ShapeDtypeStruct((NSTATE, length), BF16),
            jax.ShapeDtypeStruct((heads, length), F32),
            jax.ShapeDtypeStruct((heads, 1), F32),
        ),
        in_specs=vmem_specs(11),
        out_specs=tuple(vmem_specs(5)),
        scratch_shapes=[
            VMEM((heads, length), F32),
            VMEM((heads, length, LANES), F32),
            VMEM((length, length), F32),
            VMEM((NSTATE, length), BF16),
        ],
        name="span",
        cost_estimate=cost(10**10, 4 * 10**6),
    )(
        x_in, rims[:value_rows], conv_x,
        b_own, rims[value_rows : value_rows + NSTATE], taps_b,
        c_own, rims[value_rows + NSTATE :], taps_c,
        dt_raw, decay_rate.reshape(heads, 1),
    )

    def passed(state, reach, steps):
        moved = from_behind(state.astype(BF16), "ep", steps).astype(F32)
        return moved, from_behind(reach, "ep", steps)

    state, reach = passed(state.reshape(heads, HEAD_DIM, NSTATE), reach, 1)
    steps = 1
    while steps < ep_size - 1:
        before, before_reach = passed(state, reach, steps)
        state = state + reach[:, :, None] * before
        reach = reach * before_reach
        steps *= 2
    incoming = state.reshape(value_rows, NSTATE).astype(BF16)

    parts = {0: arrived}
    bit = tp_size // 2
    while bit:
        parts.update({part | bit: swap(parts[part], "tp", bit) for part in list(parts)})
        bit //= 2
    hidden_units = w_gate.shape[2]
    tile = 256 if hidden_units % 256 == 0 else hidden_units if hidden_units % LANES else LANES
    if hidden_units < 1024:
        tile = hidden_units
    outs = pl.pallas_call(
        functools.partial(ffn_kernel, tp_size),
        grid=(hidden_units // tile,),
        out_shape=[jax.ShapeDtypeStruct((slots, width), BF16)] * tp_size,
        in_specs=vmem_specs(tp_size)
        + [
            pl.BlockSpec((1, features, tile), lambda i: (0, 0, i)),
            pl.BlockSpec((1, features, tile), lambda i: (0, 0, i)),
            pl.BlockSpec((1, tile, features), lambda i: (0, i, 0)),
        ],
        out_specs=vmem_specs(tp_size),
        scratch_shapes=[VMEM((slots, features), BF16), VMEM((slots, features), F32)],
        compiler_params=pltpu.CompilerParams(dimension_semantics=("arbitrary",), vmem_limit_bytes=56 * 2**20),
        name="ffn",
        cost_estimate=cost(6 * slots * features * hidden_units, 6 * features * hidden_units),
    )(*[parts[part] for part in range(tp_size)], w_gate, w_up, w_down)
    sums = dict(enumerate(outs))
    bit = 1
    while bit < tp_size:
        received = {part: swap(sums[part], "tp", bit) for part in sums if part & bit}
        sums = {
            part: (sums[part].astype(F32) + received[part | bit].astype(F32)).astype(BF16)
            for part in sums
            if not part & bit
        }
        bit *= 2
    returned = lax.all_to_all(
        sums[0].reshape(experts, capacity, width), "ep", split_axis=0, concat_axis=0, tiled=True
    ).reshape(slots, width)

    mixed = pl.pallas_call(
        close_kernel,
        out_shape=jax.ShapeDtypeStruct((value_rows, length), BF16),
        in_specs=vmem_specs(6),
        out_specs=pl.BlockSpec(memory_space=VMEM),
        name="close",
        cost_estimate=cost(4 * 10**9, 4 * 10**6),
    )(y_local, incoming, c_conv, cum, z_in, head_gain.reshape(value_rows, 1))
    moe_out = pl.pallas_call(
        combine_kernel,
        out_shape=jax.ShapeDtypeStruct((width, tokens), BF16),
        in_specs=vmem_specs(2),
        out_specs=pl.BlockSpec(memory_space=VMEM),
        name="combine",
        cost_estimate=cost(2 * slots * tokens * width, 2 * slots * width),
    )(returned, pick)
    return (mixed, moe_out)


def solution(mesh):
    return jax.shard_map(
        on_device,
        mesh=mesh,
        in_specs=(
            P("tp", "ep"), P("tp", "ep"), P("tp", "ep"), P("tp"), P(None, "ep"), P(None, "ep"),
            P("tp", None), P(), P(), P("tp"), P("ep", None), P(), P("ep", None), P("ep", None),
            P("ep", None, "tp"), P("ep", None, "tp"), P("ep", "tp", None),
        ),
        out_specs=(P("tp", "ep"), P("tp", "ep")),
        check_vma=False,
    )
```

time: 213 us -> 166 us (0.78)
  matrix products: 55.1 us -> 0 us
  Pallas kernels: 0 us -> 41.1 us
  other arithmetic: 25 us -> 4.11 us
  waiting for transfers between devices: 38.7 us -> 57.4 us
  blocking collectives: 38.3 us -> 21.3 us
  starting transfers between devices: 12.3 us -> 28.8 us
  between operations: 16.7 us -> 0.86 us
  local copies, waits for them, and re-layouts: 23.1 us -> 11.2 us
    ppermute x1 -> x14, waiting for transfers between devices: 0.91 us -> 57.4 us  [the longest x8 44.6 us: from_behind(): lax.ppermute(value, axis, [(source, source + steps) for source in range(c...]
    dot_general x15 -> x0, matrix products: 55.1 us -> none  [the longest x1 15.2 us: experts_half(): lax.dot_general(columns, hidden, (((0,), (1,)), ((), ())), preferred_elem...]
    pallas_call x0 -> x5, Pallas kernels: none -> 41.1 us  [the longest x1 18.7 us: on_device(): pl.pallas_call(functools.partial(ffn_kernel, tp_size), grid=(hidden_units...]
    all_gather x2 -> x0, waiting for transfers between devices: 37.8 us -> none  [the longest x1 24.8 us: carried_in(): lax.all_gather(a.astype(kind), axis)]
    unnamed x1 -> x0, blocking collectives: 17.1 us -> none
    ppermute x1 -> x14, starting transfers between devices: 3.31 us -> 19.7 us  [the longest x8 16.3 us: from_behind(): lax.ppermute(value, axis, [(source, source + steps) for source in range(c...]
    add x6 -> x0, other arithmetic: 6.77 us -> none  [combine_states(): after_part[0][..., None, None] * before_part[1] + after_part[1]]
    dynamic_slice x18 -> x2, local copies, waits for them, and re-layouts: 7.23 us -> 0.72 us  [of_group(): return lax.dynamic_slice_in_dim(tensor, group * NSTATE, NSTATE, 0)]
  transfers between devices with their start and end apart: 5 -> 15, of which waited for: 3 -> 6; matrix products, arithmetic and copies ran while one was open for 32% -> 7% of each run, Pallas kernels for 0% -> 10%
where the time goes in v1:
time: 166 us; the launch traced here: 165 us
  waiting for transfers between devices  57.4 us (35%)
  Pallas kernels  41.1 us (25%)
  starting transfers between devices  28.8 us (17%)
  blocking collectives  21.3 us (13%)
  local copies, waits for them, and re-layouts  11.2 us (7%)
  other arithmetic  4.11 us (2%)
    ppermute x8, waiting for transfers between devices, from_behind(): lax.ppermute(value, axis, [(source, source + steps) for source in range(c...  44.6 us
    all_to_all x1, blocking collectives, on_device(): lax.all_to_all(outbox.reshape(experts, capacity, width), 'ep', split_axis...  21.3 us
    pallas_call x1, Pallas kernels, on_device(): pl.pallas_call(functools.partial(ffn_kernel, tp_size), grid=(hidden_units...  18.7 us
    ppermute x8, starting transfers between devices, from_behind(): lax.ppermute(value, axis, [(source, source + steps) for source in range(c...  16.3 us
    ppermute x6, waiting for transfers between devices, swap(): lax.ppermute(value, axis, [(source, source ^ bit) for source in range(cou...  12.8 us
    pallas_call x1, Pallas kernels, on_device(): pl.pallas_call(span_kernel, out_shape=(jax.ShapeDtypeStruct((value_rows,...  11.4 us
    all_to_all x1, starting transfers between devices, on_device(): lax.all_to_all(sums[0].reshape(experts, capacity, width), 'ep', split_axi...  9.04 us
    unnamed x34, local copies, waits for them, and re-layouts  5.96 us
  transfers between devices with their start and end apart: 15, of which 6 were waited for; matrix products, arithmetic and copies ran while one was open for 7% of the time, Pallas kernels for 10%

profile of v1, /device:TPU:24, one launch (start us, length us, event | category | flops | bytes accessed | tf_op | source)
XLA Modules:
  0.0 164.8 jit_solution(16658225137528631300)
XLA Ops:
  0.7 3.0 %outbox.1 = (bf16[640,512]{1,0:T(8,128)(2,1)}, bf16[640,160]{1,0:T(8,128)(2,1)}) custom-call(bf16[160,2048]{1,0:T(8,128)(2,1)} %rows_ref.1, f32[1,2048]{1,0:T(1,128)} %bitcast.23, s32[2,160]{1,0:T(2,128)} %bitcast.25, f32[2,160]{1,0:T(2,128)} %bitcast.26), custom_call_target="tpu_custom_call" | custom-call | flops 104857600 | bytes 655360 | tf_op jit(solution)/shard_map/outbox/pallas_call | solution.py:220
  3.6 21.3 %all_to_all.10 = bf16[8,80,512]{2,1,0:T(8,128)(2,1)S(1)} all-to-all(bf16[8,80,512]{2,1,0:T(8,128)(2,1)} %bitcast.20), channel_id=1, replica_groups=mesh['ep'=8,'tp'=4] {'ep'}, dimensions={0} | all-to-all | bytes 1310720 | tf_op jit(solution)/shard_map/all_to_all | solution.py:231
  25.0 1.5 collective-permute-start.9
  26.7 1.1 slice.18
  27.9 12.8 %collective-permute-done.9.refs_2_ = bf16[640,512]{1,0:T(8,128)(2,1)S(1)} collective-permute-done((bf16[640,512]{1,0:T(8,128)(2,1)S(1)}, bf16[640,512]{1,0:T(8,128)(2,1)S(1)}, u32[]{:S(2)}, u32[]{:S(2)}) %collective-permute-start.9) | collective-permute-done | bytes 655392 | tf_op jit(solution)/shard_map/ppermute | solution.py:201
  40.7 3.8 %collective-permute-start = (bf16[3,1280]{0,1:T(8,128)(2,1)S(1)}, bf16[3,1280]{0,1:T(8,128)(2,1)S(1)}, u32[]{:S(2)}, u32[]{:S(2)}) collective-permute-start(bf16[3,1280]{0,1:T(8,128)(2,1)S(1)} %maximum_bitcast_fusion), channel_id=1, source_target_pairs={{0,4},{4,8},{8,12},{12,16},{16,20},{20,24},{24,28},{1,5},{5,9},{9,... | collective-permute-start | bytes 23048 | tf_op jit(solution)/shard_map/ppermute | solution.py:196
  46.7 1.0 copy.42.tapx_ref
  48.4 5.2 %collective-permute-done = bf16[3,1280]{0,1:T(8,128)(2,1)S(1)} collective-permute-done((bf16[3,1280]{0,1:T(8,128)(2,1)S(1)}, bf16[3,1280]{0,1:T(8,128)(2,1)S(1)}, u32[]{:S(2)}, u32[]{:S(2)}) %collective-permute-start) | collective-permute-done | bytes 7712 | tf_op jit(solution)/shard_map/ppermute | solution.py:196
  54.4 0.8 pad_slice_fusion.2.rim_ref
  56.0 18.7 %ffn.1 = (bf16[640,512]{1,0:T(8,128)(2,1)}, bf16[640,512]{1,0:T(8,128)(2,1)}, bf16[640,512]{1,0:T(8,128)(2,1)}, bf16[640,512]{1,0:T(8,128)(2,1)}) custom-call(bf16[640,512]{1,0:T(8,128)(2,1)} %bitcast.19, bf16[640,512]{1,0:T(8,128)(2,1)} %copy-done.13, bf16[640,512]{1,0:T(8,128)(2,1)} %copy-done.11, bf16[640,512]{1,0:T(8,128)(2,1)} %collective-permute-done.10.refs_3_, ...), custom_call_target="tpu_custom_call" | custom-call | flops 10066329600 | bytes 15728640 | tf_op jit(solution)/shard_map/ffn/pallas_call | solution.py:293
  74.7 11.4 %span.1 = (f32[1024,384]{1,0:T(8,128)}, f32[1024,128]{1,0:T(8,128)}, bf16[128,384]{1,0:T(8,128)(2,1)}, f32[16,384]{1,0:T(8,128)}, f32[16,1]{1,0:T(8,128)}) custom-call(bf16[1024,384]{1,0:T(8,128)(2,1)} %x_ref.1, bf16[1024,128]{1,0:T(8,128)(2,1)} %pad_slice_fusion.2.rim_ref, f32[1024,4]{1,0:T(8,128)} %copy.42.tapx_ref, ...), custom_call_target="tpu_custom_call" | custom-call | flops 10000000000 | bytes 4000000 | tf_op jit(solution)/shard_map/span/pallas_call | solution.py:245
  86.1 1.1 convert_element_type.59
  87.2 2.9 %collective-permute-start.1 = (bf16[16,64,128]{2,1,0:T(8,128)(2,1)S(1)}, bf16[16,64,128]{2,1,0:T(8,128)(2,1)S(1)}, u32[]{:S(2)}, u32[]{:S(2)}) collective-permute-start(bf16[16,64,128]{2,1,0:T(8,128)(2,1)S(1)} %bitcast.21), channel_id=1, source_target_pairs={{0,4},{4,8},{8,12},{12,16},{16,20},{20,24},{24,28},{1,5},{5,9},{9,... | collective-permute-start | bytes 786440 | tf_op jit(solution)/shard_map/ppermute | solution.py:196
  90.6 1.6 collective-permute-start.13
  92.2 6.6 %collective-permute-done.1 = bf16[16,64,128]{2,1,0:T(8,128)(2,1)S(1)} collective-permute-done((bf16[16,64,128]{2,1,0:T(8,128)(2,1)S(1)}, bf16[16,64,128]{2,1,0:T(8,128)(2,1)S(1)}, u32[]{:S(2)}, u32[]{:S(2)}) %collective-permute-start.1) | collective-permute-done | bytes 262176 | tf_op jit(solution)/shard_map/ppermute | solution.py:196
  98.7 2.0 %collective-permute-start.3 = (bf16[16,64,128]{2,1,0:T(8,128)(2,1)S(1)}, bf16[16,64,128]{2,1,0:T(8,128)(2,1)S(1)}, u32[]{:S(2)}, u32[]{:S(2)}) collective-permute-start(bf16[16,64,128]{2,1,0:T(8,128)(2,1)S(1)} %collective-permute-done.1), channel_id=1, source_target_pairs={{0,4},{4,8},{8,12},{12,16},{16,20},{20,24},{24,28},{1,5},{5,9},{9,... | collective-permute-start | bytes 786440 | tf_op jit(solution)/shard_map/ppermute | solution.py:196
  100.7 1.9 %collective-permute-start.2 = (f32[16,1]{1,0:T(8,128)S(1)}, f32[16,1]{1,0:T(8,128)S(1)}, u32[]{:S(2)}, u32[]{:S(2)}) collective-permute-start(f32[16,1]{1,0:T(8,128)S(1)} %copy-done.14), channel_id=1, source_target_pairs={{0,4},{4,8},{8,12},{12,16},{16,20},{20,24},{24,28},{1,5},{5,9},{9,... | collective-permute-start | bytes 200 | tf_op jit(solution)/shard_map/ppermute | solution.py:196
  102.6 6.9 %collective-permute-done.2 = f32[16,1]{1,0:T(8,128)S(1)} collective-permute-done((f32[16,1]{1,0:T(8,128)S(1)}, f32[16,1]{1,0:T(8,128)S(1)}, u32[]{:S(2)}, u32[]{:S(2)}) %collective-permute-start.2) | collective-permute-done | bytes 96 | tf_op jit(solution)/shard_map/ppermute | solution.py:196
  109.5 1.9 %collective-permute-start.4 = (f32[16,1]{1,0:T(8,128)S(1)}, f32[16,1]{1,0:T(8,128)S(1)}, u32[]{:S(2)}, u32[]{:S(2)}) collective-permute-start(f32[16,1]{1,0:T(8,128)S(1)} %collective-permute-done.2), channel_id=1, source_target_pairs={{0,4},{4,8},{8,12},{12,16},{16,20},{20,24},{24,28},{1,5},{5,9},{9,... | collective-permute-start | bytes 200 | tf_op jit(solution)/shard_map/ppermute | solution.py:196
  111.4 4.5 %collective-permute-done.4 = f32[16,1]{1,0:T(8,128)S(1)} collective-permute-done((f32[16,1]{1,0:T(8,128)S(1)}, f32[16,1]{1,0:T(8,128)S(1)}, u32[]{:S(2)}, u32[]{:S(2)}) %collective-permute-start.4) | collective-permute-done | bytes 96 | tf_op jit(solution)/shard_map/ppermute | solution.py:196
  116.1 1.3 collective-permute-start.6
  117.5 1.3 collective-permute-start.5
  118.9 1.1 add_convert_fusion
  120.0 9.0 %all-to-all-start.1 = ((bf16[8,80,512]{2,1,0:T(8,128)(2,1)}), bf16[8,80,512]{2,1,0:T(8,128)(2,1)S(1)}, u32[]{:S(2)}, u32[]{:S(2)}) async-start(bf16[8,80,512]{2,1,0:T(8,128)(2,1)} %bitcast.11), calls=%async_computation.1 | async-start | bytes 1310720 | tf_op jit(solution)/shard_map/all_to_all | solution.py:319
  129.4 1.3 collective-permute-start.7
  130.7 1.0 copy.44.gain_ref
  131.8 21.4 %collective-permute-done.7 = bf16[16,64,128]{2,1,0:T(8,128)(2,1)S(1)} collective-permute-done((bf16[16,64,128]{2,1,0:T(8,128)(2,1)S(1)}, bf16[16,64,128]{2,1,0:T(8,128)(2,1)S(1)}, u32[]{:S(2)}, u32[]{:S(2)}) %collective-permute-start.7) | collective-permute-done | bytes 262176 | tf_op jit(solution)/shard_map/ppermute | solution.py:196
  153.2 1.0 add_convert_fusion.3
  154.2 5.8 %close.1 = bf16[1024,384]{1,0:T(8,128)(2,1)} custom-call(f32[1024,384]{1,0:T(8,128)} %get-tuple-element.13.y_ref, bf16[1024,128]{1,0:T(8,128)(2,1)} %bitcast.22, bf16[128,384]{1,0:T(8,128)(2,1)} %get-tuple-element.16.conv_ref, f32[16,384]{1,0:T(8,128)} %get-tuple-element.17.cum_ref, bf16[1024,384]{1,0:T(8,128)(2,1)} %z_ref.1, f32[1024,1]{1,0:T(8,128)} %copy.44.gain_ref), custom_call_target="tpu_custom_call" | custom-call | flops 4000000000 | bytes 4000000 | tf_op jit(solution)/shard_map/close/pallas_call | solution.py:323
  160.0 0.8 copy-done
  160.8 2.3 %combine.1 = bf16[512,160]{1,0:T(8,128)(2,1)} custom-call(bf16[640,512]{1,0:T(8,128)(2,1)} %bitcast.14, bf16[640,160]{1,0:T(8,128)(2,1)} %get-tuple-element.23.pick_ref), custom_call_target="tpu_custom_call" | custom-call | flops 104857600 | bytes 655360 | tf_op jit(solution)/shard_map/combine/pallas_call | solution.py:331
  163.1 1.7 %copy.45 = bf16[512,160]{0,1:T(8,128)(2,1)} copy(bf16[512,160]{1,0:T(8,128)(2,1)} %combine.1) | data formatting | bytes 327680
  (56 shorter events, 5.9 us)
Async XLA Ops:
  0.6 25.9 %copy-start.5 = (bf16[256,384]{1,0:T(8,128)(2,1)S(1)}, bf16[256,384]{1,0:T(8,128)(2,1)}, u32[]{:S(2)}) copy-start(bf16[256,384]{1,0:T(8,128)(2,1)} %param.21) | copy-start | bytes 589828
  0.6 26.0 %copy-start.4 = (bf16[256,384]{1,0:T(8,128)(2,1)S(1)}, bf16[256,384]{1,0:T(8,128)(2,1)}, u32[]{:S(2)}) copy-start(bf16[256,384]{1,0:T(8,128)(2,1)} %param.22) | copy-start | bytes 589828
  3.6 41.6 %copy-start.8 = (f32[256,4]{0,1:T(4,128)S(1)}, f32[256,4]{0,1:T(4,128)}, u32[]{:S(2)}) copy-start(f32[256,4]{0,1:T(4,128)} %param.25) | copy-start | bytes 12292
  3.6 41.6 %copy-start.9 = (f32[256,4]{0,1:T(4,128)S(1)}, f32[256,4]{0,1:T(4,128)}, u32[]{:S(2)}) copy-start(f32[256,4]{0,1:T(4,128)} %param.24) | copy-start | bytes 12292
  3.6 43.1 %copy-start.6 = (f32[1024,4]{0,1:T(4,128)S(1)}, f32[1024,4]{0,1:T(4,128)}, u32[]{:S(2)}) copy-start(f32[1024,4]{0,1:T(4,128)} %param.23) | copy-start | bytes 49156
  25.0 29.4 %copy-start.2 = (bf16[8,80,512]{2,1,0:T(8,128)(2,1)}, bf16[8,80,512]{2,1,0:T(8,128)(2,1)S(1)}, u32[]{:S(2)}) copy-start(bf16[8,80,512]{2,1,0:T(8,128)(2,1)S(1)} %all_to_all.10) | copy-start | bytes 1966084
  25.0 22.7 %copy-start.10 = (f32[16]{0:T(128)S(1)}, f32[16]{0:T(128)}, u32[]{:S(2)}) copy-start(f32[16]{0:T(128)} %param.20) | copy-start | bytes 196
  25.0 15.7 %collective-permute-start.9 = (bf16[640,512]{1,0:T(8,128)(2,1)S(1)}, bf16[640,512]{1,0:T(8,128)(2,1)S(1)}, u32[]{:S(2)}, u32[]{:S(2)}) collective-permute-start(bf16[640,512]{1,0:T(8,128)(2,1)S(1)} %bitcast.17), channel_id=1, source_target_pairs={{0,2},{1,3},{2,0},{3,1},{4,6},{5,7},{6,4},{7,5},{8,10},{9,11},{10,... | collective-permute-start | bytes 1966088 | tf_op jit(solution)/shard_map/ppermute | solution.py:201
  27.8 27.4 %collective-permute-start.8 = (bf16[640,512]{1,0:T(8,128)(2,1)S(1)}, bf16[640,512]{1,0:T(8,128)(2,1)S(1)}, u32[]{:S(2)}, u32[]{:S(2)}) collective-permute-start(bf16[640,512]{1,0:T(8,128)(2,1)S(1)} %bitcast.18), channel_id=1, source_target_pairs={{0,1},{1,0},{2,3},{3,2},{4,5},{5,4},{6,7},{7,6},{8,9},{9,8},{10,11... | collective-permute-start | bytes 1966088 | tf_op jit(solution)/shard_map/ppermute | solution.py:201
  40.7 14.6 %copy-start.11 = (bf16[640,512]{1,0:T(8,128)(2,1)}, bf16[640,512]{1,0:T(8,128)(2,1)S(1)}, u32[]{:S(2)}) copy-start(bf16[640,512]{1,0:T(8,128)(2,1)S(1)} %collective-permute-done.9.refs_2_) | copy-start | bytes 1966084
  40.7 14.6 %collective-permute-start.10 = (bf16[640,512]{1,0:T(8,128)(2,1)S(1)}, bf16[640,512]{1,0:T(8,128)(2,1)}, u32[]{:S(2)}, u32[]{:S(2)}) collective-permute-start(bf16[640,512]{1,0:T(8,128)(2,1)S(1)} %collective-permute-done.9.refs_2_), channel_id=1, source_target_pairs={{0,1},{1,0},{2,3},{3,2},{4,5},{5,4},{6,7},{7,6},{8,9},{9,8},{10,11... | collective-permute-start | bytes 1966088 | tf_op jit(solution)/shard_map/ppermute | solution.py:201
  40.7 12.9 %collective-permute-start = (bf16[3,1280]{0,1:T(8,128)(2,1)S(1)}, bf16[3,1280]{0,1:T(8,128)(2,1)S(1)}, u32[]{:S(2)}, u32[]{:S(2)}) collective-permute-start(bf16[3,1280]{0,1:T(8,128)(2,1)S(1)} %maximum_bitcast_fusion), channel_id=1, source_target_pairs={{0,4},{4,8},{8,12},{12,16},{16,20},{20,24},{24,28},{1,5},{5,9},{9,... | collective-permute-start | bytes 23048 | tf_op jit(solution)/shard_map/ppermute | solution.py:196
  55.2 0.8 copy-start.13
  74.7 15.7 %collective-permute-start.12 = (bf16[640,512]{1,0:T(8,128)(2,1)}, bf16[640,512]{1,0:T(8,128)(2,1)S(1)}, u32[]{:S(2)}, u32[]{:S(2)}) collective-permute-start(bf16[640,512]{1,0:T(8,128)(2,1)} %get-tuple-element.22), channel_id=1, source_target_pairs={{0,1},{1,0},{2,3},{3,2},{4,5},{5,4},{6,7},{7,6},{8,9},{9,8},{10,11... | collective-permute-start | bytes 1966088 | tf_op jit(solution)/shard_map/ppermute | solution.py:201
  74.7 15.4 %copy-start.12 = (bf16[640,512]{1,0:T(8,128)(2,1)S(1)}, bf16[640,512]{1,0:T(8,128)(2,1)}, u32[]{:S(2)}) copy-start(bf16[640,512]{1,0:T(8,128)(2,1)} %get-tuple-element.20) | copy-start | bytes 1966084
  74.7 15.7 %copy-start.3 = (bf16[640,512]{1,0:T(8,128)(2,1)S(1)}, bf16[640,512]{1,0:T(8,128)(2,1)}, u32[]{:S(2)}) copy-start(bf16[640,512]{1,0:T(8,128)(2,1)} %get-tuple-element.21) | copy-start | bytes 1966084
  86.1 14.6 %copy-start.14 = (f32[16,1]{1,0:T(8,128)S(1)}, f32[16,1]{1,0:T(8,128)}, u32[]{:S(2)}) copy-start(f32[16,1]{1,0:T(8,128)} %get-tuple-element.15) | copy-start | bytes 196
  87.2 11.5 %collective-permute-start.1 = (bf16[16,64,128]{2,1,0:T(8,128)(2,1)S(1)}, bf16[16,64,128]{2,1,0:T(8,128)(2,1)S(1)}, u32[]{:S(2)}, u32[]{:S(2)}) collective-permute-start(bf16[16,64,128]{2,1,0:T(8,128)(2,1)S(1)} %bitcast.21), channel_id=1, source_target_pairs={{0,4},{4,8},{8,12},{12,16},{16,20},{20,24},{24,28},{1,5},{5,9},{9,... | collective-permute-start | bytes 786440 | tf_op jit(solution)/shard_map/ppermute | solution.py:196
  90.1 28.7 %collective-permute-start.11 = (bf16[640,512]{1,0:T(8,128)(2,1)S(1)}, bf16[640,512]{1,0:T(8,128)(2,1)S(1)}, u32[]{:S(2)}, u32[]{:S(2)}) collective-permute-start(bf16[640,512]{1,0:T(8,128)(2,1)S(1)} %copy-done.12), channel_id=1, source_target_pairs={{0,1},{1,0},{2,3},{3,2},{4,5},{5,4},{6,7},{7,6},{8,9},{9,8},{10,11... | collective-permute-start | bytes 1966088 | tf_op jit(solution)/shard_map/ppermute | solution.py:201
  90.4 28.5 %copy-start.1 = (bf16[640,512]{1,0:T(8,128)(2,1)S(1)}, bf16[640,512]{1,0:T(8,128)(2,1)}, u32[]{:S(2)}) copy-start(bf16[640,512]{1,0:T(8,128)(2,1)} %get-tuple-element.19) | copy-start | bytes 1966084
  90.6 28.3 %collective-permute-start.13 = (bf16[640,512]{1,0:T(8,128)(2,1)S(1)}, bf16[640,512]{1,0:T(8,128)(2,1)S(1)}, u32[]{:S(2)}, u32[]{:S(2)}) collective-permute-start(bf16[640,512]{1,0:T(8,128)(2,1)S(1)} %add_convert_fusion.1), channel_id=1, source_target_pairs={{0,2},{1,3},{2,0},{3,1},{4,6},{5,7},{6,4},{7,5},{8,10},{9,11},{10,... | collective-permute-start | bytes 1966088 | tf_op jit(solution)/shard_map/ppermute | solution.py:201
  98.7 18.6 %collective-permute-start.3 = (bf16[16,64,128]{2,1,0:T(8,128)(2,1)S(1)}, bf16[16,64,128]{2,1,0:T(8,128)(2,1)S(1)}, u32[]{:S(2)}, u32[]{:S(2)}) collective-permute-start(bf16[16,64,128]{2,1,0:T(8,128)(2,1)S(1)} %collective-permute-done.1), channel_id=1, source_target_pairs={{0,4},{4,8},{8,12},{12,16},{16,20},{20,24},{24,28},{1,5},{5,9},{9,... | collective-permute-start | bytes 786440 | tf_op jit(solution)/shard_map/ppermute | solution.py:196
  100.7 8.8 %collective-permute-start.2 = (f32[16,1]{1,0:T(8,128)S(1)}, f32[16,1]{1,0:T(8,128)S(1)}, u32[]{:S(2)}, u32[]{:S(2)}) collective-permute-start(f32[16,1]{1,0:T(8,128)S(1)} %copy-done.14), channel_id=1, source_target_pairs={{0,4},{4,8},{8,12},{12,16},{16,20},{20,24},{24,28},{1,5},{5,9},{9,... | collective-permute-start | bytes 200 | tf_op jit(solution)/shard_map/ppermute | solution.py:196
  109.5 6.4 %collective-permute-start.4 = (f32[16,1]{1,0:T(8,128)S(1)}, f32[16,1]{1,0:T(8,128)S(1)}, u32[]{:S(2)}, u32[]{:S(2)}) collective-permute-start(f32[16,1]{1,0:T(8,128)S(1)} %collective-permute-done.2), channel_id=1, source_target_pairs={{0,4},{4,8},{8,12},{12,16},{16,20},{20,24},{24,28},{1,5},{5,9},{9,... | collective-permute-start | bytes 200 | tf_op jit(solution)/shard_map/ppermute | solution.py:196
  116.1 13.0 %collective-permute-start.6 = (f32[16,1]{1,0:T(8,128)S(1)}, f32[16,1]{1,0:T(8,128)S(1)}, u32[]{:S(2)}, u32[]{:S(2)}) collective-permute-start(f32[16,1]{1,0:T(8,128)S(1)} %get-tuple-element.36), channel_id=1, source_target_pairs={{0,8},{4,12},{8,16},{12,20},{16,24},{20,28},{1,9},{5,13},{9,17},{1... | collective-permute-start | bytes 200 | tf_op jit(solution)/shard_map/ppermute | solution.py:196
  117.5 11.6 %collective-permute-start.5 = (bf16[16,64,128]{2,1,0:T(8,128)(2,1)S(1)}, bf16[16,64,128]{2,1,0:T(8,128)(2,1)S(1)}, u32[]{:S(2)}, u32[]{:S(2)}) collective-permute-start(bf16[16,64,128]{2,1,0:T(8,128)(2,1)S(1)} %fusion), channel_id=1, source_target_pairs={{0,8},{4,12},{8,16},{12,20},{16,24},{20,28},{1,9},{5,13},{9,17},{1... | collective-permute-start | bytes 786440 | tf_op jit(solution)/shard_map/ppermute | solution.py:196
  120.0 10.7 %copy-start.7 = (f32[1024]{0:T(1024)S(1)}, f32[1024]{0:T(1024)}, u32[]{:S(2)}) copy-start(f32[1024]{0:T(1024)} %param.26) | copy-start | bytes 12292
  120.0 40.0 %all-to-all-start.1 = ((bf16[8,80,512]{2,1,0:T(8,128)(2,1)}), bf16[8,80,512]{2,1,0:T(8,128)(2,1)S(1)}, u32[]{:S(2)}, u32[]{:S(2)}) async-start(bf16[8,80,512]{2,1,0:T(8,128)(2,1)} %bitcast.11), calls=%async_computation.1 | async-start | bytes 1310720 | tf_op jit(solution)/shard_map/all_to_all | solution.py:319
  129.4 23.7 %collective-permute-start.7 = (bf16[16,64,128]{2,1,0:T(8,128)(2,1)S(1)}, bf16[16,64,128]{2,1,0:T(8,128)(2,1)S(1)}, u32[]{:S(2)}, u32[]{:S(2)}) collective-permute-start(bf16[16,64,128]{2,1,0:T(8,128)(2,1)S(1)} %fusion.1), channel_id=1, source_target_pairs={{0,16},{4,20},{8,24},{12,28},{1,17},{5,21},{9,25},{13,29},{2,18},{... | collective-permute-start | bytes 786440 | tf_op jit(solution)/shard_map/ppermute | solution.py:196
  160.0 0.8 copy-start

commit v2 on v1

v2 whole, which is shorter than its diff:
```python
import functools
import jax
import jax.numpy as jnp
from jax import lax
from jax.experimental import pallas as pl
from jax.experimental.pallas import tpu as pltpu
from jax.sharding import PartitionSpec as P

HEADS = 64
HEAD_DIM = 64
GROUPS = 2
NSTATE = 128
BLOCK = 128
ROW_EPS = 0.1
HEAD_EPS = 1.0
LANES = 128
F32 = jnp.float32
BF16 = jnp.bfloat16
VMEM = pltpu.VMEM
MESH = pl.DeviceIdType.MESH


def vmem_specs(count):
    return [pl.BlockSpec(memory_space=VMEM)] * count


def cost(flops, moved):
    return pl.CostEstimate(flops=flops, bytes_accessed=moved, transcendentals=0)


def dot(a, b, dims, precision=None):
    return lax.dot_general(a, b, (dims, ((), ())), preferred_element_type=F32, precision=precision)


def eye(count):
    row = lax.broadcasted_iota(jnp.int32, (count, count), 0)
    col = lax.broadcasted_iota(jnp.int32, (count, count), 1)
    return jnp.where(row == col, 1.0, 0.0).astype(F32)


def upright(flat):
    return dot(flat, eye(flat.shape[0]), ((0,), (0,)), lax.Precision.HIGHEST)


def silu(v):
    return v / (1.0 + jnp.exp(-v))


def conv_rows(signal, rim, weight):
    taps = weight.shape[1]
    joined = jnp.concatenate([rim.astype(F32), signal.astype(F32)], axis=1)
    running = weight[:, taps - 1 : taps] * joined[:, LANES:]
    for back in range(1, taps):
        moved = pltpu.roll(joined, back, 1)[:, LANES:]
        running = running + weight[:, taps - 1 - back : taps - back] * moved
    return silu(running)


def prefix_decays(dt_ref, rate_ref):
    dt = dt_ref[...]
    step = jnp.maximum(dt, 0.0) + jnp.log1p(jnp.exp(-jnp.abs(dt)))
    rate = jnp.where(eye(dt.shape[0]) > 0.0, rate_ref[...], 0.0)
    log_decay = -step * jnp.sum(rate, axis=1, keepdims=True)
    length = dt.shape[1]
    row = lax.broadcasted_iota(jnp.int32, (length, length), 0)
    col = lax.broadcasted_iota(jnp.int32, (length, length), 1)
    upper = jnp.where(row <= col, 1.0, 0.0).astype(F32)
    lower = jnp.where(row >= col, 1.0, 0.0).astype(F32)
    high = lax.Precision.HIGHEST
    cum = dot(log_decay, upper, ((1,), (0,)), high)
    cum_col = dot(lower, log_decay, ((1,), (1,)), high)
    return step, cum, cum_col


def flip(place, mask):
    bit = 1
    while bit <= mask:
        if mask & bit:
            place = place + bit * (1 - 2 * ((place // bit) % 2))
        bit *= 2
    return place


def greet(ep_size, tp_size):
    barrier = pltpu.get_barrier_semaphore()
    me, lane = lax.axis_index("ep"), lax.axis_index("tp")
    count = 0
    for hop in range(1, ep_size):
        pl.semaphore_signal(barrier, 1, device_id={"ep": (me + hop) % ep_size}, device_id_type=MESH)
        count += 1
    bit = 1
    while bit < tp_size:
        pl.semaphore_signal(barrier, 1, device_id={"tp": flip(lane, bit)}, device_id_type=MESH)
        count += 1
        bit *= 2
    pl.semaphore_wait(barrier, count)


def remote(source, target, send, recv, **where):
    return pltpu.make_async_remote_copy(
        src_ref=source, dst_ref=target, send_sem=send, recv_sem=recv, device_id=where, device_id_type=MESH
    )


class Prefix:
    def __init__(self, state, reach, out, out_reach, got, got_reach, send, recv, ep_size):
        self.state, self.reach = state, reach
        self.out, self.out_reach, self.got, self.got_reach = out, out_reach, got, got_reach
        self.send, self.recv, self.size = send, recv, ep_size

    def copies(self, turn, steps):
        target = (lax.axis_index("ep") + steps) % self.size
        return (
            remote(self.out.at[turn], self.got.at[turn], self.send.at[turn, 0], self.recv.at[turn, 0], ep=target),
            remote(self.out_reach.at[turn], self.got_reach.at[turn], self.send.at[turn, 1], self.recv.at[turn, 1], ep=target),
        )

    def begin(self, turn, steps):
        me = lax.axis_index("ep")

        @pl.when(me + steps < self.size)
        def _():
            self.out[turn] = self.state[...].astype(BF16)
            self.out_reach[turn] = self.reach[...]
            for copy in self.copies(turn, steps):
                copy.start()

    def finish(self, turn, steps, first):
        me = lax.axis_index("ep")

        @pl.when(me >= steps)
        def _():
            for copy in self.copies(turn, steps):
                copy.wait_recv()
            if first:
                self.state[...] = self.got[turn].astype(F32)
                self.reach[...] = self.got_reach[turn]
            else:
                for head in range(self.reach.shape[0]):
                    rows = slice(head * HEAD_DIM, (head + 1) * HEAD_DIM)
                    before = self.got[turn, rows, :].astype(F32)
                    self.state[rows, :] = self.state[rows, :] + self.reach[head : head + 1, :] * before
                self.reach[...] = self.reach[...] * self.got_reach[turn]

        if first:

            @pl.when(me < steps)
            def _():
                self.state[...] = jnp.zeros_like(self.state)
                self.reach[...] = jnp.zeros_like(self.reach)

        @pl.when(me + steps < self.size)
        def _():
            for copy in self.copies(turn, steps):
                copy.wait_send()


def spread_kernel(
    rows_ref, gain_ref, routes_ref, logit_ref, x_ref, tapx_ref, b_ref, tapb_ref, c_ref, tapc_ref, dt_ref, rate_ref,
    joined_ref, pick_ref, y_ref, state_ref, reach_ref, conv_ref, cum_ref,
    outbox, rank_ref, weight_ref, xrim, brim, crim, tap_col, tapb_col, tapc_col,
    step_ref, col_ref, score_ref, bconv_ref, out, out_reach, got, got_reach,
    rim_send, rim_recv, box_send, box_recv, ag_send, ag_recv, pre_send, pre_recv,
    *, ep_size, tp_size,
):
    me, lane = lax.axis_index("ep"), lax.axis_index("tp")
    experts, capacity, features = joined_ref.shape
    width = features // tp_size
    tokens = rows_ref.shape[0]
    heads, length = dt_ref.shape

    def cols(part):
        return pl.ds(pl.multiple_of(flip(lane, part) * width, LANES), width)

    greet(ep_size, tp_size)
    end = pl.ds(length - LANES, LANES)
    after = (me + 1) % ep_size
    rims = [
        remote(source.at[:, end], target, rim_send.at[i], rim_recv.at[i], ep=after)
        for i, (source, target) in enumerate(((x_ref, xrim), (b_ref, brim), (c_ref, crim)))
    ]

    @pl.when(me + 1 < ep_size)
    def _():
        for copy in rims:
            copy.start()

    @pl.when(me == 0)
    def _():
        for ref in (xrim, brim, crim):
            ref[...] = jnp.zeros_like(ref)

    values = rows_ref[...].astype(F32)
    scale = lax.rsqrt(jnp.mean(values * values, axis=1, keepdims=True) + ROW_EPS)
    normed = (rows_ref[:, cols(0)].astype(F32) * scale * gain_ref[:, cols(0)]).astype(BF16)
    routes = routes_ref[...]
    logit = logit_ref[...]
    first = 1.0 / (1.0 + jnp.exp(logit[1:2] - logit[0:1]))
    second = 1.0 / (1.0 + jnp.exp(logit[0:1] - logit[1:2]))
    number = lax.broadcasted_iota(jnp.int32, (experts, tokens), 0)
    in_first = number == routes[0:1]
    in_second = number == routes[1:2]
    hits = jnp.where(in_first, 1.0, 0.0) + jnp.where(in_second, 1.0, 0.0)
    row = lax.broadcasted_iota(jnp.int32, (tokens, tokens), 0)
    col = lax.broadcasted_iota(jnp.int32, (tokens, tokens), 1)
    earlier = jnp.where(row < col, 1.0, 0.0).astype(BF16)
    rank = dot(hits.astype(BF16), earlier, ((1,), (0,)))
    weight_ref[...] = jnp.where(in_first, first, 0.0) + jnp.where(in_second, second, 0.0)
    rank_ref[...] = jnp.where(hits > 0.0, rank, -1.0)
    place = lax.broadcasted_iota(jnp.int32, (capacity, tokens), 0).astype(F32)

    def box(hop):
        return remote(
            outbox.at[hop], joined_ref.at[me, :, cols(0)], box_send.at[hop], box_recv.at[hop], ep=(me + hop) % ep_size
        )

    for hop in list(range(1, ep_size)) + [0]:
        expert = (me + hop) % ep_size
        same = place == rank_ref[pl.ds(expert, 1), :]
        pick_ref[expert] = jnp.where(same, weight_ref[pl.ds(expert, 1), :], 0.0).astype(BF16)
        chosen = dot(jnp.where(same, 1.0, 0.0).astype(BF16), normed, ((1,), (0,))).astype(BF16)
        if hop:
            outbox[hop] = chosen
            box(hop).start()
        else:
            joined_ref[me, :, cols(0)] = chosen

    def passing(part, bit, hop):
        at = joined_ref.at[(me + ep_size - hop) % ep_size, :, cols(part)]
        return remote(at, at, ag_send.at[part + bit, hop], ag_recv.at[part + bit, hop], tp=flip(lane, bit))

    bits = [1 << i for i in range(tp_size.bit_length() - 1)][::-1]
    passing(0, bits[0], 0).start()

    tap_col[...] = upright(tapx_ref[...])
    tapb_col[...] = upright(tapb_ref[...])
    tapc_col[...] = upright(tapc_ref[...])
    step, cum, cum_col = prefix_decays(dt_ref, rate_ref)
    step_ref[...] = step
    cum_ref[...] = cum
    reach_ref[...] = jnp.broadcast_to(jnp.exp(cum[:, length - 1 :]), reach_ref.shape)
    for head in range(heads):
        col_ref[head] = jnp.broadcast_to(cum_col[:, head : head + 1], (length, LANES))

    @pl.when(me > 0)
    def _():
        for copy in rims:
            copy.wait_recv()

    group = pl.ds(pl.multiple_of(lane * heads // (HEADS // GROUPS) * NSTATE, NSTATE), NSTATE)
    b_conv = conv_rows(b_ref[group, :], brim[group, :], tapb_col[group, :]).astype(BF16)
    c_conv = conv_rows(c_ref[group, :], crim[group, :], tapc_col[group, :]).astype(BF16)
    bconv_ref[...] = b_conv
    conv_ref[...] = c_conv
    score_ref[...] = dot(b_conv, c_conv, ((0,), (0,)))
    brow = lax.broadcasted_iota(jnp.int32, (BLOCK, BLOCK), 0)
    bcol = lax.broadcasted_iota(jnp.int32, (BLOCK, BLOCK), 1)
    causal = brow <= bcol

    def one(head, carry):
        rows = pl.ds(pl.multiple_of(head * HEAD_DIM, HEAD_DIM), HEAD_DIM)
        x = conv_rows(x_ref[rows, :], xrim[rows, :], tap_col[rows, :])
        own = cum_ref[pl.ds(head, 1), :]
        xs = x * step_ref[pl.ds(head, 1), :]
        tail = xs * jnp.exp(own[:, length - 1 :] - own)
        state_ref[rows, :] = dot(tail.astype(BF16), bconv_ref[...], ((1,), (1,)))
        xs = xs.astype(BF16)
        for target in range(length // BLOCK):
            at = slice(target * BLOCK, (target + 1) * BLOCK)
            pieces = []
            for source in range(target + 1):
                of = slice(source * BLOCK, (source + 1) * BLOCK)
                gap = own[:, at] - col_ref[head, of, :]
                if source == target:
                    gap = jnp.where(causal, gap, -jnp.inf)
                pieces.append((score_ref[of, at] * jnp.exp(gap)).astype(BF16))
            mask = pieces[0] if target == 0 else jnp.concatenate(pieces, axis=0)
            y_ref[rows, at] = dot(xs[:, : (target + 1) * BLOCK], mask, ((1,), (0,)))
        return carry

    lax.fori_loop(0, heads * 3 // 4, one, 0)
    for hop in range(1, ep_size):
        if hop == ep_size // 2:
            lax.fori_loop(heads * 3 // 4, heads, one, 0)
            chain = Prefix(
                state_ref, reach_ref, out, out_reach, got, got_reach, pre_send, pre_recv, ep_size
            )
            chain.begin(0, 1)
        box(hop).wait_recv()
        passing(0, bits[0], hop).start()
    have = [0]
    for index, bit in enumerate(bits):
        for hop in range(ep_size):
            passing(0, bit, hop).wait_recv()
            for part in have[1:]:
                passing(part, bit, hop).wait_recv()
            if index + 1 < len(bits):
                for part in have + [part + bit for part in have]:
                    passing(part, bits[index + 1], hop).start()
        have = have + [part + bit for part in have]
        if index == 0:
            chain.finish(0, 1, True)
            chain.begin(1, 1)
    chain.finish(1, 1, False)
    have = [0]
    for bit in bits:
        for hop in range(ep_size):
            for part in have:
                passing(part, bit, hop).wait_send()
        have = have + [part + bit for part in have]
    for hop in range(1, ep_size):
        box(hop).wait_send()

    @pl.when(me + 1 < ep_size)
    def _():
        for copy in rims:
            copy.wait_send()


def gather_kernel(
    part_ref, first_ref, first_reach,
    back_ref, state_ref,
    sums, landed, final, reach_ref, out, out_reach, got, got_reach,
    rs_send, rs_recv, box_send, box_recv, pre_send, pre_recv,
    *, ep_size, tp_size, rounds,
):
    me, lane = lax.axis_index("ep"), lax.axis_index("tp")
    width = part_ref.shape[2] // tp_size
    greet(ep_size, tp_size)
    bits = [1 << i for i in range(tp_size.bit_length() - 1)]
    order = list(range(1, ep_size)) + [0]

    def cols(part):
        return pl.ds(pl.multiple_of(flip(lane, part) * width, LANES), width)

    def passing(part, bit, hop):
        chunk = (me + hop) % ep_size
        source = part_ref.at[chunk, :, cols(part)] if bit == 1 else sums.at[part, chunk]
        return remote(source, landed.at[part, chunk], rs_send.at[part, hop], rs_recv.at[part, hop], tp=flip(lane, bit))

    def box(hop):
        return remote(final.at[hop], back_ref.at[me], box_send.at[hop], box_recv.at[hop], ep=(me + hop) % ep_size)

    for hop in order:
        for part in range(1, tp_size, 2):
            passing(part, 1, hop).start()
    state_ref[...] = first_ref[...]
    reach_ref[...] = first_reach[...]
    chain = Prefix(state_ref, reach_ref, out, out_reach, got, got_reach, pre_send, pre_recv, ep_size)
    if rounds:
        chain.begin(0, rounds[0])
    done = 0
    for bit in bits:
        kept = range(0, tp_size, 2 * bit)
        for hop in order:
            chunk = (me + hop) % ep_size
            for part in list(kept)[::-1]:
                passing(part + bit, bit, hop).wait_recv()
                mine = part_ref[chunk, :, cols(part)] if bit == 1 else sums[part, chunk]
                total = (mine.astype(F32) + landed[part + bit, chunk].astype(F32)).astype(BF16)
                if bit < bits[-1]:
                    sums[part, chunk] = total
                    if part & (2 * bit):
                        passing(part, 2 * bit, hop).start()
                elif hop:
                    final[hop] = total
                    box(hop).start()
                else:
                    back_ref[me] = total
        if done < len(rounds):
            chain.finish(done, rounds[done], False)
            done += 1
            if done < len(rounds):
                chain.begin(done, rounds[done])
    while done < len(rounds):
        chain.finish(done, rounds[done], False)
        done += 1
        if done < len(rounds):
            chain.begin(done, rounds[done])
    for hop in range(1, ep_size):
        box(hop).wait_recv()
        box(hop).wait_send()
    for bit in bits:
        for part in range(bit, tp_size, 2 * bit):
            for hop in order:
                passing(part, bit, hop).wait_send()


def close_kernel(y_ref, state_ref, conv_ref, cum_ref, z_ref, gain_ref, out_ref, gain_col):
    heads = cum_ref.shape[0]
    top = lax.broadcasted_iota(jnp.int32, (8, LANES), 0) == 0
    flat = jnp.broadcast_to(gain_ref[...], (8, gain_ref.shape[1]))
    gain_col[...] = dot(flat, jnp.where(top, 1.0, 0.0), ((0,), (0,)), lax.Precision.HIGHEST)

    def one(head, carry):
        rows = pl.ds(pl.multiple_of(head * HEAD_DIM, HEAD_DIM), HEAD_DIM)
        carried = dot(state_ref[rows, :].astype(BF16), conv_ref[...], ((1,), (0,)))
        y = y_ref[rows, :] + carried * jnp.exp(cum_ref[pl.ds(head, 1), :])
        gated = y * silu(z_ref[rows, :].astype(F32))
        scale = lax.rsqrt(jnp.mean(gated * gated, axis=0, keepdims=True) + HEAD_EPS)
        out_ref[rows, :] = (gated * scale * gain_col[rows, 0:1]).astype(BF16)
        return carry

    lax.fori_loop(0, heads, one, 0)


def ffn_kernel(joined, gate_ref, up_ref, down_ref, out_ref, total):
    turn = pl.program_id(0)
    gate = dot(joined[...], gate_ref[0], ((1,), (0,)))
    up = dot(joined[...], up_ref[0], ((1,), (0,)))
    hidden = (silu(gate) * up).astype(BF16)
    partial = dot(hidden, down_ref[0], ((1,), (0,)))

    @pl.when(turn == 0)
    def _():
        total[...] = partial

    @pl.when(turn > 0)
    def _():
        total[...] += partial

    @pl.when(turn == pl.num_programs(0) - 1)
    def _():
        out_ref[...] = total[...].astype(BF16)


def combine_kernel(back_ref, pick_ref, out_ref):
    out_ref[...] = dot(pick_ref[...], back_ref[...], ((0,), (0,))).astype(BF16)


def on_device(
    x_in, z_in, dt_raw, decay_rate, b_in, c_in, conv_x, conv_b, conv_c, head_gain,
    moe_rows, moe_gain, routes, route_logit, w_gate, w_up, w_down,
):
    heads, length = dt_raw.shape
    value_rows = x_in.shape[0]
    taps = conv_x.shape[1]
    tp_size = lax.axis_size("tp")
    ep_size = lax.axis_size("ep")
    tokens, features = moe_rows.shape
    experts = ep_size
    capacity = 2 * tokens * routes.shape[1] // experts
    width = features // tp_size
    slots = experts * capacity
    dma = pltpu.SemaphoreType.DMA
    shape = jax.ShapeDtypeStruct

    def chain(turns):
        return [
            VMEM((turns, value_rows, NSTATE), BF16),
            VMEM((turns, heads, NSTATE), F32),
            VMEM((turns, value_rows, NSTATE), BF16),
            VMEM((turns, heads, NSTATE), F32),
        ]

    joined, pick, y_local, state, reach, c_conv, cum = pl.pallas_call(
        functools.partial(spread_kernel, ep_size=ep_size, tp_size=tp_size),
        out_shape=(
            shape((experts, capacity, features), BF16),
            shape((experts, capacity, tokens), BF16),
            shape((value_rows, length), F32),
            shape((value_rows, NSTATE), F32),
            shape((heads, NSTATE), F32),
            shape((NSTATE, length), BF16),
            shape((heads, length), F32),
        ),
        in_specs=vmem_specs(12),
        out_specs=tuple(vmem_specs(7)),
        scratch_shapes=[
            VMEM((experts, capacity, width), BF16),
            VMEM((experts, tokens), F32),
            VMEM((experts, tokens), F32),
            VMEM((value_rows, LANES), BF16),
            VMEM((b_in.shape[0], LANES), BF16),
            VMEM((c_in.shape[0], LANES), BF16),
            VMEM((value_rows, taps), F32),
            VMEM((b_in.shape[0], taps), F32),
            VMEM((c_in.shape[0], taps), F32),
            VMEM((heads, length), F32),
            VMEM((heads, length, LANES), F32),
            VMEM((length, length), F32),
            VMEM((NSTATE, length), BF16),
        ]
        + chain(2)
        + [
            dma((3,)), dma((3,)), dma((ep_size,)), dma((ep_size,)),
            dma((tp_size, ep_size)), dma((tp_size, ep_size)), dma((2, 2)), dma((2, 2)),
        ],
        compiler_params=pltpu.CompilerParams(collective_id=0, has_side_effects=True, vmem_limit_bytes=48 * 2**20),
        name="spread",
    )(
        moe_rows, moe_gain.reshape(1, features), routes.T, route_logit.T,
        x_in, conv_x.T, b_in, conv_b.T, c_in, conv_c.T, dt_raw, decay_rate.reshape(1, heads),
    )

    hidden_units = w_gate.shape[2]
    tile = hidden_units if hidden_units < 1024 else 256
    partial = pl.pallas_call(
        ffn_kernel,
        grid=(hidden_units // tile,),
        out_shape=shape((slots, features), BF16),
        in_specs=vmem_specs(1)
        + [
            pl.BlockSpec((1, features, tile), lambda i: (0, 0, i)),
            pl.BlockSpec((1, features, tile), lambda i: (0, 0, i)),
            pl.BlockSpec((1, tile, features), lambda i: (0, i, 0)),
        ],
        out_specs=pl.BlockSpec(memory_space=VMEM),
        scratch_shapes=[VMEM((slots, features), F32)],
        compiler_params=pltpu.CompilerParams(dimension_semantics=("arbitrary",), vmem_limit_bytes=48 * 2**20),
        name="ffn",
    )(joined.reshape(slots, features), w_gate, w_up, w_down)

    rounds = []
    steps = 2
    while steps < ep_size - 1:
        rounds.append(steps)
        steps *= 2
    turns = max(1, len(rounds))
    returned, incoming = pl.pallas_call(
        functools.partial(gather_kernel, ep_size=ep_size, tp_size=tp_size, rounds=rounds),
        out_shape=(shape((experts, capacity, width), BF16), shape((value_rows, NSTATE), F32)),
        in_specs=vmem_specs(3),
        out_specs=tuple(vmem_specs(2)),
        scratch_shapes=[
            VMEM((tp_size, experts, capacity, width), BF16),
            VMEM((tp_size, experts, capacity, width), BF16),
            VMEM((experts, capacity, width), BF16),
            VMEM((heads, NSTATE), F32),
        ]
        + chain(turns)
        + [
            dma((tp_size, ep_size)), dma((tp_size, ep_size)), dma((ep_size,)), dma((ep_size,)),
            dma((turns, 2)), dma((turns, 2)),
        ],
        compiler_params=pltpu.CompilerParams(collective_id=1, has_side_effects=True, vmem_limit_bytes=48 * 2**20),
        name="gather",
    )(partial.reshape(experts, capacity, features), state, reach)

    mixed = pl.pallas_call(
        close_kernel,
        out_shape=shape((value_rows, length), BF16),
        in_specs=vmem_specs(6),
        out_specs=pl.BlockSpec(memory_space=VMEM),
        scratch_shapes=[VMEM((value_rows, LANES), F32)],
        name="close",
    )(y_local, incoming, c_conv, cum, z_in, head_gain.reshape(1, value_rows))
    moe_out = pl.pallas_call(
        combine_kernel,
        out_shape=shape((tokens, width), BF16),
        in_specs=vmem_specs(2),
        out_specs=pl.BlockSpec(memory_space=VMEM),
        name="combine",
    )(returned.reshape(slots, width), pick.reshape(slots, tokens))
    return (mixed, moe_out.T)


def solution(mesh):
    return jax.shard_map(
        on_device,
        mesh=mesh,
        in_specs=(
            P("tp", "ep"), P("tp", "ep"), P("tp", "ep"), P("tp"), P(None, "ep"), P(None, "ep"),
            P("tp", None), P(), P(), P("tp"), P("ep", None), P(), P("ep", None), P("ep", None),
            P("ep", None, "tp"), P("ep", None, "tp"), P("ep", "tp", None),
        ),
        out_specs=(P("tp", "ep"), P("tp", "ep")),
        check_vma=False,
    )
```

time: 166 us -> 122 us (0.73)
  Pallas kernels: 41.1 us -> 104 us
  waiting for transfers between devices: 57.4 us -> 0 us
  starting transfers between devices: 28.8 us -> 0 us
  blocking collectives: 21.3 us -> 0 us
  local copies, waits for them, and re-layouts: 11.2 us -> 15.5 us
  other arithmetic: 4.11 us -> 0 us
    pallas_call x5, Pallas kernels: 41.1 us -> 104 us  [the longest x1 44.6 us: on_device(): pl.pallas_call(functools.partial(spread_kernel, ep_size=ep_size, tp_size=...]
    ppermute x14 -> x0, waiting for transfers between devices: 57.4 us -> none  [the longest x8 44.6 us: from_behind(): lax.ppermute(value, axis, [(source, source + steps) for source in range(c...]
    all_to_all x1 -> x0, blocking collectives: 21.3 us -> none  [on_device(): lax.all_to_all(outbox.reshape(experts, capacity, width), 'ep', split_axis...]
    ppermute x14 -> x0, starting transfers between devices: 19.7 us -> none  [the longest x8 16.3 us: from_behind(): lax.ppermute(value, axis, [(source, source + steps) for source in range(c...]
    unnamed x34 -> x38, local copies, waits for them, and re-layouts: 5.96 us -> 15.5 us
    all_to_all x1 -> x0, starting transfers between devices: 9.04 us -> none  [on_device(): lax.all_to_all(sums[0].reshape(experts, capacity, width), 'ep', split_axi...]
    convert_element_type x6 -> x0, other arithmetic: 3.82 us -> none  [the longest x3 1.51 us: passed(): moved = from_behind(state.astype(BF16), 'ep', steps).astype(F32)]
    slice x5 -> x0, local copies, waits for them, and re-layouts: 2.81 us -> none  [the longest x1 1.08 us: on_device(): x_in[:, edge:]]
  transfers between devices with their start and end apart: 15 -> 0, of which waited for: 6 -> 0; matrix products, arithmetic and copies ran while one was open for 7% -> 0% of each run, Pallas kernels for 10% -> 0%
where the time goes in v2:
time: 122 us; the launch traced here: 120 us
  Pallas kernels  104 us (85%)
  local copies, waits for them, and re-layouts  15.5 us (13%)
    pallas_call x1, Pallas kernels, on_device(): pl.pallas_call(functools.partial(spread_kernel, ep_size=ep_size, tp_size=...  44.6 us
    pallas_call x1, Pallas kernels, on_device(): pl.pallas_call(functools.partial(gather_kernel, ep_size=ep_size, tp_size=...  35.3 us
    pallas_call x1, Pallas kernels, on_device(): pl.pallas_call(ffn_kernel, grid=(hidden_units // tile,), out_shape=shape(...  15.7 us
    unnamed x38, local copies, waits for them, and re-layouts  15.5 us
    pallas_call x1, Pallas kernels, on_device(): pl.pallas_call(close_kernel, out_shape=shape((value_rows, length), BF16),...  6.28 us

profile of v2, /device:TPU:24, one launch (start us, length us, event | category | flops | bytes accessed | tf_op | source)
XLA Modules:
  0.0 120.3 jit_solution(17231439424381460881)
XLA Ops:
  0.6 0.0 copy-start.2
  0.6 1.1 copy-done.2
  1.8 0.0 copy-start.3
  1.8 1.1 copy-done.3
  2.9 0.0 copy-start.7
  2.9 0.9 copy-done.7
  3.8 0.0 copy-start.8
  3.8 0.9 copy-done.8
  4.7 0.0 copy-start.10
  4.7 0.7 copy-done.10
  5.4 0.0 copy-start.12
  5.5 0.7 copy-done.12
  6.2 0.7 copy-done.13
  6.9 0.7 copy-done.14
  7.6 0.7 copy-done.15
  8.2 0.7 copy-done.16
  8.9 0.7 copy-done.17
  9.6 0.7 copy-done.18
  10.3 44.6 %spread.1 = (bf16[8,80,2048]{2,1,0:T(8,128)(2,1)}, bf16[8,80,160]{2,1,0:T(8,128)(2,1)S(1)}, f32[1024,384]{1,0:T(8,128)S(1)}, f32[1024,128]{1,0:T(8,128)S(1)}, f3...) custom-call(bf16[160,2048]{1,0:T(8,128)(2,1)S(1)} %copy-done.3, f32[1,2048]{1,0:T(1,128)S(1)} %bitcast.18, ...), custom_call_target="tpu_custom_call" | custom-call | tf_op jit(solution)/shard_map/spread/pallas_call | solution.py:456
  54.9 0.0 copy-start.1
  54.9 1.1 copy-done.1
  56.0 0.7 copy-done.6
  56.8 0.6 copy-done.9
  57.4 1.7 %copy-done = bf16[8,80,2048]{2,1,0:T(8,128)(2,1)S(1)} copy-done((bf16[8,80,2048]{2,1,0:T(8,128)(2,1)S(1)}, bf16[8,80,2048]{2,1,0:T(8,128)(2,1)}, u32[]{:S(2)}) %copy-start) | copy-done | bytes 2621464
  59.2 15.7 %ffn.1 = bf16[640,2048]{1,0:T(8,128)(2,1)S(1)} custom-call(bf16[640,2048]{1,0:T(8,128)(2,1)S(1)} %bitcast.14, bf16[1,2048,1280]{2,1,0:T(8,128)(2,1)} %gate_ref.1, bf16[1,2048,1280]{2,1,0:T(8,128)(2,1)} %up_ref.1, bf16[1,1280,2048]{2,1,0:T(8,128)(2,1)} %down_ref.1), custom_call_target="tpu_custom_call" | custom-call | tf_op jit(solution)/shard_map/ffn/pallas_call | solution.py:498
  74.9 0.0 copy-done.11
  74.9 35.3 %gather.1 = (bf16[8,80,512]{2,1,0:T(8,128)(2,1)S(1)}, f32[1024,128]{1,0:T(8,128)S(1)}) custom-call(bf16[8,80,2048]{2,1,0:T(8,128)(2,1)S(1)} %bitcast.13, f32[1024,128]{1,0:T(8,128)S(1)} %get-tuple-element.13.first_ref, f32[16,128]{1,0:T(8,128)S(1)} %get-tuple-element.14.first_reach), custom_call_target="tpu_custom_call" | custom-call | tf_op jit(solution)/shard_map/gather/pallas_call | solution.py:520
  110.2 0.0 copy-start.4
  110.3 0.8 copy-done.4
  111.1 0.8 copy-done.5
  111.9 6.3 %close.1 = bf16[1024,384]{1,0:T(8,128)(2,1)} custom-call(f32[1024,384]{1,0:T(8,128)} %copy-done.1, f32[1024,128]{1,0:T(8,128)} %copy-done.5, bf16[128,384]{1,0:T(8,128)(2,1)} %copy-done.9, f32[16,384]{1,0:T(8,128)} %copy-done.11, bf16[1024,384]{1,0:T(8,128)(2,1)} %z_ref.1, f32[1,1024]{1,0:T(1,128)} %bitcast.25), custom_call_target="tpu_custom_call" | custom-call | tf_op jit(solution)/shard_map/close/pallas_call | solution.py:540
  118.2 2.2 %combine.1 = bf16[160,512]{1,0:T(8,128)(2,1)} custom-call(bf16[640,512]{1,0:T(8,128)(2,1)} %bitcast.15, bf16[640,160]{1,0:T(8,128)(2,1)} %bitcast.16), custom_call_target="tpu_custom_call" | custom-call | tf_op jit(solution)/shard_map/combine/pallas_call | solution.py:548
  (11 shorter events, 0.0 us)
Async XLA Ops:
  0.6 1.1 copy-start.2
  1.8 1.1 copy-start.3
  2.9 0.9 copy-start.7
  3.8 0.9 copy-start.8
  4.7 0.7 copy-start.10
  5.4 0.7 copy-start.12
  6.2 0.7 copy-start.13
  6.9 0.7 copy-start.14
  7.6 0.7 copy-start.15
  8.2 0.7 copy-start.16
  8.9 0.7 copy-start.17
  9.6 0.7 copy-start.18
  54.9 1.2 copy-start.1
  56.0 0.7 copy-start.6
  56.8 0.6 copy-start.9
  57.4 17.5 %copy-start.11 = (f32[16,384]{1,0:T(8,128)}, f32[16,384]{1,0:T(8,128)S(1)}, u32[]{:S(2)}) copy-start(f32[16,384]{1,0:T(8,128)S(1)} %get-tuple-element.17.cum_ref) | copy-start | bytes 73732
  57.4 1.8 %copy-start = (bf16[8,80,2048]{2,1,0:T(8,128)(2,1)S(1)}, bf16[8,80,2048]{2,1,0:T(8,128)(2,1)}, u32[]{:S(2)}) copy-start(bf16[8,80,2048]{2,1,0:T(8,128)(2,1)} %get-tuple-element.12) | copy-start | bytes 7864324
  110.2 0.8 copy-start.4
  111.1 0.8 copy-start.5
